TPU v7x, 128 devices: a whole 4x4x4 slice. The times are simulated.
128 devices in a mesh: sp: 16 (over z, y), dp: 8 (over x, core).
Axes of the slice: x: 4, y: 4, z: 4, core: 2. Of those that a mesh axis runs over, the one named last changes fastest.
Arguments:
- queries: bfloat16 [8, 2048, 1024], P('dp', 'sp'), may hold values from -6 to 6
- keys: bfloat16 [8, 2048, 256], P('dp', 'sp'), may hold values from -6 to 6
- values: bfloat16 [8, 2048, 256], P('dp', 'sp'), may hold values from -6 to 6
- q_gain: float32 [64], replicated, may hold values from 0.55 to 8
- k_gain: float32 [64], replicated, may hold values from 0.55 to 8
- residual: bfloat16 [8, 2048, 2048], P('dp', 'sp'), may hold values from -6 to 6
- out_weight: bfloat16 [1024, 2048], replicated, may hold values from -0.1875 to 0.1875
- mix_gain: float32 [2048], replicated, may hold values from 0.1 to 1.9
- ffn_gain: float32 [2048], replicated, may hold values from 0.1 to 1.9
- post_gain: float32 [2048], replicated, may hold values from 0.1 to 1.9
- expert_ids: int32 [8, 2048, 2], P('dp', 'sp'), may hold values from 0 to 127, all different within a row; in each aligned block of 128 rows (0 to 127, 128 to 255, ..., all dimensions but the last counted through in order) at most 4 rows name the same one
- expert_gate: float32 [8, 2048, 2], P('dp', 'sp'), may hold values from 0.05 to 1
- w_gate: bfloat16 [128, 2048, 512], P(('sp', 'dp')), may hold values from -0.125 to 0.125
- w_up: bfloat16 [128, 2048, 512], P(('sp', 'dp')), may hold values from -0.125 to 0.125
- w_down: bfloat16 [128, 512, 2048], P(('sp', 'dp')), may hold values from -0.25 to 0.25
Outputs:
- result: bfloat16 [8, 2048, 2048], P('dp', 'sp')
Inputs may be any that keep to these rules, and one draw needn't show every extreme that they name: `expert_ids`: each token names 2 different experts; among the 128 tokens of one device no expert is named more than 4 times, and that bound is reached.
All inputs are finite; a program needn't handle non-finite values.
Results may differ from a plain program's by a relative error of at most 0.0085.
The roundings to bfloat16 on the way count: a program that leaves them out, or rounds other values in their place, can miss the bound.
Values may be sent and summed in bfloat16 or wider, within the bound.
A program may use at most 64 MiB of HBM per device.

v0:
```python
import jax
import jax.numpy as jnp
from jax import lax
from jax.sharding import PartitionSpec as P

D = 2048
GRID = 64


eps_norm = 1e-06
theta_base = 10000.0
block_rows = 512


def rms_scale(values):
    return values * lax.rsqrt(jnp.mean(values * values, axis=-1, keepdims=True) + eps_norm)


def rotate(field, gain):
    seq_len, head_count, head_size = field.shape
    values = rms_scale(field.astype(jnp.float32)) * gain
    positions = jnp.arange(seq_len, dtype=jnp.int32)
    row_index = (positions // GRID).astype(jnp.float32)
    col_index = (positions % GRID).astype(jnp.float32)
    pair_quarter = head_size // 4
    frequency = theta_base ** (-(4.0 * jnp.arange(pair_quarter, dtype=jnp.float32)) / head_size)
    angles = jnp.concatenate(
        [row_index[:, None] * frequency, col_index[:, None] * frequency], axis=1
    )
    cosine_table = jnp.cos(angles)[:, None, :]
    sine_table = jnp.sin(angles)[:, None, :]
    paired = values.reshape(seq_len, head_count, head_size // 2, 2)
    even_part = paired[..., 0]
    odd_part = paired[..., 1]
    turned = jnp.stack(
        [
            even_part * cosine_table - odd_part * sine_table,
            even_part * sine_table + odd_part * cosine_table,
        ],
        axis=-1,
    )
    return turned.reshape(seq_len, head_count, head_size).astype(jnp.bfloat16)


def attend(q_turned, k_turned, v_rows):
    seq_len, q_count, head_size = q_turned.shape
    kv_count = k_turned.shape[1]
    group_size = q_count // kv_count

    def one_block(start):
        q_block = lax.dynamic_slice_in_dim(q_turned, start, block_rows, 0)
        q_block = q_block.reshape(block_rows, kv_count, group_size, head_size)
        scores = jnp.einsum(
            "qkgd,skd->kgqs", q_block, k_turned, preferred_element_type=jnp.float32
        ) * head_size ** (-0.5)
        row_max = jnp.max(scores, axis=-1, keepdims=True)
        exp_scores = jnp.exp(scores - row_max)
        weights = (exp_scores / jnp.sum(exp_scores, axis=-1, keepdims=True)).astype(jnp.bfloat16)
        summed = jnp.einsum("kgqs,skd->qkgd", weights, v_rows, preferred_element_type=jnp.float32)
        return summed.astype(jnp.bfloat16).reshape(block_rows, q_count * head_size)

    starts = jnp.arange(seq_len // block_rows, dtype=jnp.int32) * block_rows
    return lax.map(one_block, starts).reshape(seq_len, q_count * head_size)


def shards(
    queries,
    keys,
    values,
    q_gain,
    k_gain,
    residual,
    out_weight,
    mix_gain,
    ffn_gain,
    post_gain,
    expert_ids,
    expert_gate,
    w_gate,
    w_up,
    w_down,
):
    sp_count = lax.axis_size("sp")
    dp_count = lax.axis_size("dp")
    tok_rows = queries.shape[1]
    head_size = q_gain.shape[0]
    heads_q = queries.shape[2] // head_size
    heads_kv = keys.shape[2] // head_size
    q_here = heads_q // sp_count
    kv_here = max(q_here * heads_kv // heads_q, 1)
    copies = kv_here * sp_count // heads_kv
    key_rows = jnp.repeat(keys[0].reshape(tok_rows, heads_kv, head_size), copies, axis=1).reshape(
        tok_rows, -1
    )
    value_rows = jnp.repeat(
        values[0].reshape(tok_rows, heads_kv, head_size), copies, axis=1
    ).reshape(tok_rows, -1)
    q_heads, k_heads, v_heads = (
        lax.all_to_all(queries[0], "sp", split_axis=1, concat_axis=0, tiled=True),
        lax.all_to_all(key_rows, "sp", split_axis=1, concat_axis=0, tiled=True),
        lax.all_to_all(value_rows, "sp", split_axis=1, concat_axis=0, tiled=True),
    )
    seq_len = q_heads.shape[0]
    q_turned = rotate(q_heads.reshape(seq_len, q_here, head_size), q_gain)
    k_turned = rotate(k_heads.reshape(seq_len, kv_here, head_size), k_gain)
    attended = attend(q_turned, k_turned, v_heads.reshape(seq_len, kv_here, head_size))
    token_side = lax.all_to_all(attended, "sp", split_axis=0, concat_axis=1, tiled=True)
    projected = jnp.dot(token_side, out_weight, preferred_element_type=jnp.float32)
    first_res = (residual[0].astype(jnp.float32) + rms_scale(projected) * mix_gain).astype(
        jnp.bfloat16
    )
    normed = (rms_scale(first_res.astype(jnp.float32)) * ffn_gain).astype(jnp.bfloat16)
    experts_all = sp_count * dp_count
    top_n = expert_ids.shape[2]
    capacity = 2 * tok_rows * top_n // experts_all
    flat_ids = expert_ids[0].reshape(-1)
    onehot = (flat_ids[:, None] == jnp.arange(experts_all, dtype=jnp.int32)[None, :]).astype(
        jnp.int32
    )
    running = jnp.cumsum(onehot, axis=0) - onehot
    slot_index = jnp.sum(running * onehot, axis=1)
    target = flat_ids * capacity + slot_index
    sources = jnp.repeat(normed, top_n, axis=0)
    outbox = jnp.zeros((experts_all * capacity, D), jnp.bfloat16).at[target].set(sources)
    outbox = outbox.reshape(experts_all, capacity, D)
    arrived = lax.all_to_all(outbox, ("sp", "dp"), split_axis=0, concat_axis=0, tiled=True)
    layout = arrived.shape
    flattened = arrived.reshape(-1, layout[-1])
    gate_value = jnp.dot(flattened, w_gate[0], preferred_element_type=jnp.float32)
    up_value = jnp.dot(flattened, w_up[0], preferred_element_type=jnp.float32)
    hidden = (jax.nn.silu(gate_value) * up_value).astype(jnp.bfloat16)
    answer = jnp.dot(hidden, w_down[0], preferred_element_type=jnp.float32).astype(jnp.bfloat16)
    returned = lax.all_to_all(
        answer.reshape(layout), ("sp", "dp"), split_axis=0, concat_axis=0, tiled=True
    )
    flat_back = returned.reshape(experts_all * capacity, D)
    answers = flat_back[target].astype(jnp.float32).reshape(tok_rows, top_n, D)
    expert_sum = jnp.sum(answers * expert_gate[0][:, :, None], axis=1)
    result = (first_res.astype(jnp.float32) + rms_scale(expert_sum) * post_gain).astype(
        jnp.bfloat16
    )
    return result[None]


def solution(mesh):
    return jax.shard_map(
        shards,
        mesh=mesh,
        in_specs=(
            P("dp", "sp", None),
            P("dp", "sp", None),
            P("dp", "sp", None),
            P(),
            P(),
            P("dp", "sp", None),
            P(),
            P(),
            P(),
            P(),
            P("dp", "sp", None),
            P("dp", "sp", None),
            P(("sp", "dp"), None, None),
            P(("sp", "dp"), None, None),
            P(("sp", "dp"), None, None),
        ),
        out_specs=P("dp", "sp", None),
        check_vma=False,
    )
```

profile of v0, /device:TPU:0, one launch (start us, length us, event | category | flops | bytes accessed | tf_op | source)
XLA Modules:
  0.0 207.3 jit_solution(11319161728944544260)
XLA Ops:
  1.9 8.2 %all-to-all-start.1 = ((bf16[128,16,64]{0,2,1:T(8,128)(2,1)}), bf16[128,16,64]{0,2,1:T(8,128)(2,1)S(1)}, u32[]{:S(2)}, u32[]{:S(2)}) async-start(bf16[128,16,64]{0,2,1:T(8,128)(2,1)} %bitcast.20), calls=%async_computation.1 | async-start | bytes 524288 | tf_op jit(solution)/shard_map/all_to_all | solution.py:100
  14.6 4.1 %all-to-all-done.1 = bf16[128,16,64]{0,2,1:T(8,128)(2,1)S(1)} async-done(((bf16[128,16,64]{0,2,1:T(8,128)(2,1)}), bf16[128,16,64]{0,2,1:T(8,128)(2,1)S(1)}, u32[]{:S(2)}, u32[]{:S(2)}) %all-to-all-start.1) | async-done | bytes 262176 | tf_op jit(solution)/shard_map/all_to_all | solution.py:100
  18.7 3.5 %all-to-all-start = ((bf16[128,16,64]{0,2,1:T(8,128)(2,1)}), bf16[128,16,64]{0,2,1:T(8,128)(2,1)S(1)}, u32[]{:S(2)}, u32[]{:S(2)}) async-start(bf16[128,16,64]{0,2,1:T(8,128)(2,1)} %bitcast.13), calls=%async_computation | async-start | bytes 524288 | tf_op jit(solution)/shard_map/all_to_all | solution.py:99
  26.6 4.3 %all-to-all-done = bf16[128,16,64]{0,2,1:T(8,128)(2,1)S(1)} async-done(((bf16[128,16,64]{0,2,1:T(8,128)(2,1)}), bf16[128,16,64]{0,2,1:T(8,128)(2,1)S(1)}, u32[]{:S(2)}, u32[]{:S(2)}) %all-to-all-start) | async-done | bytes 262176 | tf_op jit(solution)/shard_map/all_to_all | solution.py:99
  31.7 3.5 %all-to-all-start.2 = ((bf16[128,16,64]{0,2,1:T(8,128)(2,1)}), bf16[128,16,64]{0,2,1:T(8,128)(2,1)S(1)}, u32[]{:S(2)}, u32[]{:S(2)}) async-start(bf16[128,16,64]{0,2,1:T(8,128)(2,1)} %bitcast.25), calls=%async_computation.2 | async-start | bytes 524288 | tf_op jit(solution)/shard_map/all_to_all | solution.py:101
  36.4 2.1 %reshape.537 = f32[2048,1,32,2]{0,3,2,1:T(2,128)} reshape(f32[16,128,64]{1,0,2:T(8,128)} %copy.52) | data formatting | bytes 1048576 | tf_op jit(solution)/shard_map/convert_element_type | solution.py:21
  44.2 21.6 %while.10 = (s32[]{:T(128)}, bf16[4,512,64]{1,2,0:T(8,128)(2,1)S(1)}, s32[4]{0:T(128)S(1)}, bf16[2048,1,64]{0,2,1:T(8,128)(2,1)S(1)}, bf16[2048,1,64]{0,2,1:T(8,...) while((s32[]{:T(128)}, bf16[4,512,64]{1,2,0:T(8,128)(2,1)S(1)}, ...), condition=%wide.region_5.6_spmd, body=%wide.region_2.5_spmd.sunk | while | flops 277904384 | bytes 13248659 | solution.py:63
  66.9 5.6 %all-to-all-start.3 = ((bf16[16,128,64]{1,2,0:T(8,128)(2,1)}), bf16[16,128,64]{1,2,0:T(8,128)(2,1)S(1)}, u32[]{:S(2)}, u32[]{:S(2)}) async-start(bf16[16,128,64]{1,2,0:T(8,128)(2,1)} %copy.64), calls=%async_computation.3 | async-start | bytes 524288 | tf_op jit(solution)/shard_map/all_to_all | solution.py:107
  72.9 8.2 %all-to-all-done.3 = bf16[16,128,64]{1,2,0:T(8,128)(2,1)S(1)} async-done(((bf16[16,128,64]{1,2,0:T(8,128)(2,1)}), bf16[16,128,64]{1,2,0:T(8,128)(2,1)S(1)}, u32[]{:S(2)}, u32[]{:S(2)}) %all-to-all-start.3) | async-done | bytes 262176 | tf_op jit(solution)/shard_map/all_to_all | solution.py:107
  81.2 3.1 %multiply_reduce_fusion.3 = (f32[128]{0:T(128)S(1)}, f32[128,2048]{1,0:T(8,128)S(1)}) fusion(bf16[128,1024]{0,1:T(8,128)(2,1)S(1)} %bitcast.148, bf16[1024,2048]{1,0:T(8,128)(2,1)} %param.23), kind=kOutput, calls=%fused_computation.41 | convolution fusion | flops 537395072 | bytes 5505536 | tf_op jit(solution)/shard_map/dot_general | solution.py:108
  86.8 2.3 %reshape.552 = bf16[256,2048]{1,0:T(8,128)(2,1)} reshape(bf16[128,2,2048]{2,1,0:T(2,128)(2,1)} %broadcast_in_dim.19) | data formatting | bytes 2097152 | tf_op jit(solution)/shard_map/reshape | solution.py:123
  89.0 4.4 %scatter_custom_fusion = bf16[512,2048]{1,0:T(8,128)(2,1)} fusion(s32[256]{0:T(256)S(1)} %bitcast.156, bf16[256,2048]{1,0:T(8,128)(2,1)} %reshape.552, bf16[]{:T(256)} %constant.74.clone.1), kind=kCustom, calls=%fused_computation.39 | custom fusion | bytes 2097664 | tf_op jit(solution)/shard_map/scatter | solution.py:124
  93.4 4.1 %reshape.532 = bf16[128,4,2048]{2,1,0:T(4,128)(2,1)} reshape(bf16[512,2048]{1,0:T(8,128)(2,1)} %scatter_custom_fusion) | data formatting | bytes 4194304 | tf_op jit(solution)/shard_map/reshape | solution.py:125
  97.6 36.6 %all_to_all.71 = bf16[128,4,2048]{2,1,0:T(4,128)(2,1)} all-to-all(bf16[128,4,2048]{2,1,0:T(4,128)(2,1)} %reshape.532), channel_id=1, replica_groups=mesh['sp'=16,'dp'=8] {'sp','dp'}, dimensions={0} | all-to-all | bytes 4194304 | tf_op jit(solution)/shard_map/all_to_all | solution.py:126
  134.1 4.0 %reshape.533 = bf16[512,2048]{1,0:T(8,128)(2,1)} reshape(bf16[128,4,2048]{2,1,0:T(4,128)(2,1)} %all_to_all.71) | data formatting | bytes 4194304 | tf_op jit(solution)/shard_map/reshape | solution.py:128
  138.1 4.4 %fusion.24 = f32[512,512]{1,0:T(8,128)} fusion(bf16[512,2048]{1,0:T(8,128)(2,1)} %reshape.533, bf16[1,2048,512]{2,1,0:T(8,128)(2,1)} %param.29), kind=kOutput, calls=%fused_computation.24 | convolution fusion | flops 1073741824 | bytes 5242880 | tf_op jit(solution)/shard_map/dot_general | solution.py:129
  142.5 6.2 %convolution_convert_fusion = bf16[512,2048]{1,0:T(8,128)(2,1)} fusion(bf16[1,512,2048]{2,1,0:T(8,128)(2,1)S(1)} %copy-done, bf16[512,2048]{1,0:T(8,128)(2,1)} %reshape.533, bf16[1,2048,512]{2,1,0:T(8,128)(2,1)} %param.30, f32[512,512]{1,0:T(8,128)} %fusion.24), kind=kOutput, calls=%fused_computation.20 | convolution fusion | flops 2150105088 | bytes 9437184 | tf_op jit(solution)/shard_map/dot_general | solution.py:132
  148.8 4.1 %reshape.534 = bf16[128,4,2048]{2,1,0:T(4,128)(2,1)} reshape(bf16[512,2048]{1,0:T(8,128)(2,1)} %convolution_convert_fusion) | data formatting | bytes 4194304 | tf_op jit(solution)/shard_map/reshape | solution.py:134
  152.9 6.1 %all-to-all-start.5 = ((bf16[128,4,2048]{2,1,0:T(4,128)(2,1)}), bf16[128,4,2048]{2,1,0:T(4,128)(2,1)}, u32[]{:S(2)}, u32[]{:S(2)}) async-start(bf16[128,4,2048]{2,1,0:T(4,128)(2,1)} %reshape.534), calls=%async_computation.5 | async-start | bytes 4194304 | tf_op jit(solution)/shard_map/all_to_all | solution.py:133
  159.1 29.6 %all-to-all-done.5 = bf16[128,4,2048]{2,1,0:T(4,128)(2,1)} async-done(((bf16[128,4,2048]{2,1,0:T(4,128)(2,1)}), bf16[128,4,2048]{2,1,0:T(4,128)(2,1)}, u32[]{:S(2)}, u32[]{:S(2)}) %all-to-all-start.5) | async-done | bytes 2097184 | tf_op jit(solution)/shard_map/all_to_all | solution.py:133
  188.7 4.0 %reshape.535 = bf16[512,2048]{1,0:T(8,128)(2,1)} reshape(bf16[128,4,2048]{2,1,0:T(4,128)(2,1)} %all-to-all-done.5) | data formatting | bytes 4194304 | tf_op jit(solution)/shard_map/reshape | solution.py:136
  192.7 5.2 %gather_fusion = bf16[256,2048]{1,0:T(8,128)(2,1)} fusion(bf16[512,2048]{1,0:T(8,128)(2,1)} %reshape.535, s32[1024]{0:T(1024)S(1)} %pad_clamp_fusion), kind=kCustom, calls=%fused_computation | custom fusion | bytes 2098176 | tf_op jit(solution)/shard_map/gather | solution.py:137
  197.9 3.4 %reshape.539 = f32[128,2,2048]{2,1,0:T(2,128)} reshape(bf16[256,2048]{1,0:T(8,128)(2,1)} %gather_fusion) | data formatting | bytes 3145728 | tf_op jit(solution)/shard_map/convert_element_type | solution.py:137
  201.3 4.8 %multiply_reduce_fusion.1 = f32[128,2048]{1,0:T(8,128)S(1)} fusion(f32[128,2,2048]{2,1,0:T(2,128)} %reshape.539, f32[128,2]{1,0:T(8,128)S(1)} %copy.70), kind=kLoop, calls=%fused_computation.26 | loop fusion | flops 786432 | bytes 3146752 | tf_op jit(solution)/shard_map/reduce_sum | solution.py:138
  (105 shorter events, 37.2 us)
Async XLA Ops:
  0.0 142.5 %copy-start = (bf16[1,512,2048]{2,1,0:T(8,128)(2,1)S(1)}, bf16[1,512,2048]{2,1,0:T(8,128)(2,1)}, u32[]{:S(2)}) copy-start(bf16[1,512,2048]{2,1,0:T(8,128)(2,1)} %param.31) | copy-start | bytes 6291460
  0.0 22.9 %copy-start.10 = (f32[64]{0:T(128)S(1)}, f32[64]{0:T(128)}, u32[]{:S(2)}) copy-start(f32[64]{0:T(128)} %param.20) | copy-start | bytes 772
  0.0 23.1 %copy-start.11 = (f32[64]{0:T(128)S(1)}, f32[64]{0:T(128)}, u32[]{:S(2)}) copy-start(f32[64]{0:T(128)} %param.21) | copy-start | bytes 772
  0.0 23.3 %copy-start.5 = (bf16[1,128,256]{2,1,0:T(8,128)(2,1)S(1)}, bf16[1,128,256]{2,1,0:T(8,128)(2,1)}, u32[]{:S(2)}) copy-start(bf16[1,128,256]{2,1,0:T(8,128)(2,1)} %param.19) | copy-start | bytes 196612
  1.9 16.9 %all-to-all-start.1 = ((bf16[128,16,64]{0,2,1:T(8,128)(2,1)}), bf16[128,16,64]{0,2,1:T(8,128)(2,1)S(1)}, u32[]{:S(2)}, u32[]{:S(2)}) async-start(bf16[128,16,64]{0,2,1:T(8,128)(2,1)} %bitcast.20), calls=%async_computation.1 | async-start | bytes 524288 | tf_op jit(solution)/shard_map/all_to_all | solution.py:100
  18.7 12.2 %all-to-all-start = ((bf16[128,16,64]{0,2,1:T(8,128)(2,1)}), bf16[128,16,64]{0,2,1:T(8,128)(2,1)S(1)}, u32[]{:S(2)}, u32[]{:S(2)}) async-start(bf16[128,16,64]{0,2,1:T(8,128)(2,1)} %bitcast.13), calls=%async_computation | async-start | bytes 524288 | tf_op jit(solution)/shard_map/all_to_all | solution.py:99
  31.7 12.2 %all-to-all-start.2 = ((bf16[128,16,64]{0,2,1:T(8,128)(2,1)}), bf16[128,16,64]{0,2,1:T(8,128)(2,1)S(1)}, u32[]{:S(2)}, u32[]{:S(2)}) async-start(bf16[128,16,64]{0,2,1:T(8,128)(2,1)} %bitcast.25), calls=%async_computation.2 | async-start | bytes 524288 | tf_op jit(solution)/shard_map/all_to_all | solution.py:101
  38.5 1.8 copy-start.1
  41.4 2.8 %copy-start.12 = (s32[4]{0:T(128)S(1)}, s32[4]{0:T(128)}, u32[]{:S(2)}) copy-start(s32[4]{0:T(128)} %iota_multiply_fusion) | copy-start | bytes 52
  41.5 2.7 %copy-start.4 = (bf16[4,512,64]{1,2,0:T(8,128)(2,1)S(1)}, bf16[4,512,64]{1,2,0:T(8,128)(2,1)}, u32[]{:S(2)}) copy-start(bf16[4,512,64]{1,2,0:T(8,128)(2,1)} %custom-call.2) | copy-start | bytes 786436
  65.8 6.7 %copy-start.2 = (s32[128,2,128]{0,2,1:T(8,128)S(1)}, s32[128,2,128]{0,2,1:T(8,128)}, u32[]{:S(2)}) copy-start(s32[128,2,128]{0,2,1:T(8,128)} %copy.69) | copy-start | bytes 393220
  66.9 14.3 %all-to-all-start.3 = ((bf16[16,128,64]{1,2,0:T(8,128)(2,1)}), bf16[16,128,64]{1,2,0:T(8,128)(2,1)S(1)}, u32[]{:S(2)}, u32[]{:S(2)}) async-start(bf16[16,128,64]{1,2,0:T(8,128)(2,1)} %copy.64), calls=%async_computation.3 | async-start | bytes 524288 | tf_op jit(solution)/shard_map/all_to_all | solution.py:107
  81.2 3.1 %copy-start.3 = (bf16[1,128,2048]{2,1,0:T(8,128)(2,1)S(1)}, bf16[1,128,2048]{2,1,0:T(8,128)(2,1)}, u32[]{:S(2)}) copy-start(bf16[1,128,2048]{2,1,0:T(8,128)(2,1)} %param.22) | copy-start | bytes 1572868
  81.2 3.1 %copy-start.6 = (f32[2048]{0:T(1024)S(1)}, f32[2048]{0:T(1024)}, u32[]{:S(2)}) copy-start(f32[2048]{0:T(1024)} %param.24) | copy-start | bytes 24580
  84.2 0.7 copy-start.7
  152.9 6.1 %copy-start.9 = (f32[1,128,2]{1,2,0:T(2,128)S(1)}, f32[1,128,2]{1,2,0:T(2,128)}, u32[]{:S(2)}) copy-start(f32[1,128,2]{1,2,0:T(2,128)} %param.28) | copy-start | bytes 3076
  152.9 35.8 %all-to-all-start.5 = ((bf16[128,4,2048]{2,1,0:T(4,128)(2,1)}), bf16[128,4,2048]{2,1,0:T(4,128)(2,1)}, u32[]{:S(2)}, u32[]{:S(2)}) async-start(bf16[128,4,2048]{2,1,0:T(4,128)(2,1)} %reshape.534), calls=%async_computation.5 | async-start | bytes 4194304 | tf_op jit(solution)/shard_map/all_to_all | solution.py:133
  201.3 5.0 %copy-start.8 = (f32[2048]{0:T(1024)S(1)}, f32[2048]{0:T(1024)}, u32[]{:S(2)}) copy-start(f32[2048]{0:T(1024)} %param.26) | copy-start | bytes 24580
where the time goes:
time: 209 us; the launch traced here: 207 us
  local copies, waits for them, and re-layouts  50.5 us (24%)
  waiting for transfers between devices  47.9 us (23%)
  blocking collectives  36.6 us (18%)
  starting transfers between devices  26.9 us (13%)
  matrix products  21.8 us (10%)
  other arithmetic  15.3 us (7%)
  loops' own time  7.87 us (4%)
    all_to_all x1, blocking collectives, shards(): lax.all_to_all(outbox, ('sp', 'dp'), split_axis=0, concat_axis=0, tiled=T...  36.6 us
    all_to_all x1, waiting for transfers between devices, shards(): lax.all_to_all(answer.reshape(layout), ('sp', 'dp'), split_axis=0, concat...  29.6 us
    all_to_all x1, waiting for transfers between devices, shards(): lax.all_to_all(attended, 'sp', split_axis=0, concat_axis=1, tiled=True)  8.22 us
    all_to_all x1, starting transfers between devices, shards(): lax.all_to_all(key_rows, 'sp', split_axis=1, concat_axis=0, tiled=True)  8.17 us
    another operation x1, loops' own time, attend(): return lax.map(one_block, starts).reshape(seq_len, q_count * head_size)  7.87 us
    dot_general x1, matrix products, shards(): jnp.dot(hidden, w_down[0], preferred_element_type=jnp.float32)  6.22 us
    all_to_all x1, starting transfers between devices, shards(): lax.all_to_all(answer.reshape(layout), ('sp', 'dp'), split_axis=0, concat...  6.13 us
    convert_element_type x4, local copies, waits for them, and re-layouts, rotate(): values = rms_scale(field.astype(jnp.float32)) * gain  5.61 us
  transfers between devices with their start and end apart: 5, of which 5 were waited for; matrix products, arithmetic and copies ran while one was open for 8% of the time, Pallas kernels for 0%

commit v1 on v0

v1 whole, which is shorter than its diff:
```python
import functools

import numpy as np
import jax
import jax.numpy as jnp
from jax import lax
from jax.experimental import pallas as pl
from jax.experimental.pallas import tpu as pltpu
from jax.sharding import PartitionSpec as P

MESH = pl.DeviceIdType.MESH
F32, BF16 = jnp.float32, jnp.bfloat16
EPS = 1e-06
GRID = 64
D = 2048
TOK = 128
SLOTS = 512

PARTS = (((0, 1, 2), 0, 640), ((1, 2, 0), 640, 640), ((2, 0, 1), 1280, 768))
PAIRS = ((0, 1), (1, 0))
NEAR = (1, 3, 2)
SIDES = tuple((k3, kc) for k3 in range(4) for kc in range(2) if (k3, kc) != (0, 0))


def tables():
    lane = np.arange(128) % 64
    pair = lane // 2
    freq = 10000.0 ** (-4.0 * (pair % 16) / 64.0)
    sign = np.where(lane % 2 == 0, -1.0, 1.0)
    row_lane = pair < 16
    rows = np.zeros((16, 8, 128), np.float32)
    for s in range(16):
        for i in range(2):
            ang = (2 * s + i) * freq
            rows[s, i] = np.where(row_lane, np.cos(ang), 0.0)
            rows[s, 2 + i] = np.where(row_lane, np.sin(ang) * sign, 0.0)
    ang = np.arange(64)[:, None] * freq[None, :]
    cols = np.stack(
        [np.where(row_lane, 0.0, np.cos(ang)), np.where(row_lane, 0.0, np.sin(ang) * sign)]
    ).astype(np.float32)
    return rows, cols


def rms(v):
    return v * lax.rsqrt(jnp.mean(v * v, axis=-1, keepdims=True) + EPS)


def kernel(
    q_ref, k_ref, v_ref, qg_ref, kg_ref, res_ref, wo_hbm, mix_ref, ffn_ref, post_ref,
    ids_ref, gate_ref, wg_hbm, wu_hbm, wd_hbm, rtab_ref, ctab_ref,
    out_ref,
    wo, wg, wu, wd, qp, kv, mx, acc, att, first, normed, disp, comb,
    outbox, inbox, mid, xs, ys, midr, inboxr, outr, hg, hu,
    wsem, gs, gr, f1s, f1r, f2s, f2r, f3s, f3r, r1s, r1r, r2s, r2r, r3s, r3r, own_sem,
):
    s = lax.axis_index("sp")
    d = lax.axis_index("dp")
    mine = (s // 4, s % 4, d // 2)
    core = d % 2

    def dev(axis, k, kc=0):
        p = list(mine)
        p[axis] = (p[axis] + k) % 4
        return (p[0] * 4 + p[1], p[2] * 2 + (core + kc) % 2)

    barrier = pltpu.get_barrier_semaphore()
    peers = [dev(a, k, kc) for a in range(3) for k in NEAR for kc in range(2)] + [dev(0, 0, 1)]
    for peer in peers:
        pl.semaphore_signal(barrier, 1, device_id=peer, device_id_type=MESH)

    weights = [
        pltpu.make_async_copy(src, dst, wsem.at[i])
        for i, (src, dst) in enumerate(
            ((wo_hbm, wo), (wg_hbm.at[0], wg), (wu_hbm.at[0], wu), (wd_hbm.at[0], wd))
        )
    ]
    for w in weights:
        w.start()

    lane = lax.broadcasted_iota(jnp.int32, (TOK, 128), 1)
    even = (lane % 2) == 0
    low = lane < 64
    seg = jnp.where(
        (lax.broadcasted_iota(jnp.int32, (128, 128), 0) // 64)
        == (lax.broadcasted_iota(jnp.int32, (128, 128), 1) // 64),
        1.0 / 64.0,
        0.0,
    ).astype(BF16)
    rt = rtab_ref[s]
    cos = jnp.concatenate([ctab_ref[0] + rt[0:1], ctab_ref[0] + rt[1:2]], axis=0)
    sin = jnp.concatenate([ctab_ref[1] + rt[2:3], ctab_ref[1] + rt[3:4]], axis=0)

    def turn(x, gain):
        x = x.astype(F32)
        sq = x * x
        hi = sq.astype(BF16)
        lo = (sq - hi.astype(F32)).astype(BF16)
        ms = jnp.dot(hi, seg, preferred_element_type=F32) + jnp.dot(
            lo, seg, preferred_element_type=F32
        )
        y = x * lax.rsqrt(ms + EPS) * gain
        swapped = jnp.where(even, pltpu.roll(y, 127, 1), pltpu.roll(y, 1, 1))
        return y * cos + swapped * sin

    kgain = jnp.concatenate([kg_ref[...], kg_ref[...]], axis=1)
    qgain = jnp.concatenate([qg_ref[...], qg_ref[...]], axis=1)
    for p in range(2):
        cols = slice(p * 128, (p + 1) * 128)
        kv[p, 0, :, 0:128] = turn(k_ref[0, :, cols], kgain).astype(BF16)
        kv[p, 0, :, 128:256] = v_ref[0, :, cols]
        kv[p, :, :, 256:384] = jnp.ones((16, TOK, 128), BF16)

    pl.semaphore_wait(barrier, len(peers))

    def hop(p, axis, k, src, dst):
        return pltpu.make_async_remote_copy(
            src_ref=kv.at[p, src, :, pl.ds(0, 256)],
            dst_ref=kv.at[p, dst, :, pl.ds(0, 256)],
            send_sem=gs.at[p, dst],
            recv_sem=gr.at[p, dst],
            device_id=dev(axis, k),
            device_id_type=MESH,
        )

    def gather_first(p, k1):
        return hop(p, PAIRS[p][0], k1, 0, k1)

    def gather_second(p, k2, k1):
        if k2 == 2:
            k = 1 if k1 < 2 else 3
            return hop(p, PAIRS[p][1], k, k * 4 + k1, 8 + k1)
        return hop(p, PAIRS[p][1], k2, k1, k2 * 4 + k1)

    for k1 in NEAR:
        for p in range(2):
            gather_first(p, k1).start()
    for k2 in (1, 3):
        for p in range(2):
            gather_second(p, k2, 0).start()

    for b in range(8):
        t = turn(q_ref[0, :, b * 128 : (b + 1) * 128], qgain).astype(BF16).astype(F32) * 0.125
        flip = pltpu.roll(t, 64, 1)
        p, pos, i = b // 4, (b // 2) % 2, (b % 4) * 2
        if pos == 0:
            a0, a1 = jnp.where(low, t, 0.0), jnp.where(low, flip, 0.0)
        else:
            a0, a1 = jnp.where(low, 0.0, flip), jnp.where(low, 0.0, t)
        qp[p, i * 128 : (i + 1) * 128] = a0.astype(BF16)
        qp[p, (i + 1) * 128 : (i + 2) * 128] = a1.astype(BF16)

    for k1 in NEAR:
        for p in range(2):
            gather_first(p, k1).wait_recv()
            for k2 in (1, 3):
                gather_second(p, k2, k1).start()

    tok_r = lax.broadcasted_iota(jnp.int32, (128, 128), 0)
    tok_c = lax.broadcasted_iota(jnp.int32, (128, 128), 1)
    before = (tok_r < tok_c).astype(F32).astype(BF16)
    ids = ids_ref[0].astype(F32)
    idt = [jnp.transpose(jnp.broadcast_to(ids[:, k : k + 1], (128, 128))) for k in range(2)]
    hot = [(t == tok_r.astype(F32)).astype(F32) for t in idt]
    cnt = [jnp.dot(h.astype(BF16), before, preferred_element_type=F32) for h in hot]
    cnt[1] = cnt[1] + jnp.sum(hot[0], axis=1, keepdims=True)
    rank = [jnp.sum(h * c, axis=0, keepdims=True).astype(jnp.int32) for h, c in zip(hot, cnt)]
    slot_row = lax.broadcasted_iota(jnp.int32, (SLOTS, 128), 0)
    slot_col = lax.broadcasted_iota(jnp.int32, (128, SLOTS), 1).astype(F32)
    for p, (axes, _, _) in enumerate(PARTS):
        slots = []
        for k in range(2):
            e = idt[k][0:1].astype(jnp.int32)
            at = (e // 32, (e // 8) % 4, (e // 2) % 4)
            rel = [(at[a] - mine[a] + 4) % 4 for a in axes]
            kc = (e % 2 + core) % 2
            slots.append(((rel[0] * 4 + rel[1]) * 4 + rel[2]) * 8 + kc * 4 + rank[k])
        disp[p] = ((slot_row == slots[0]) | (slot_row == slots[1])).astype(F32).astype(BF16)
        for k in range(2):
            col = jnp.transpose(jnp.broadcast_to(slots[k].astype(F32), (128, 128)))[:, 0:1]
            comb[p, k] = (slot_col == col).astype(F32).astype(BF16)

    def stripe(k2, fresh):
        for p in range(2):
            keys = kv[p, k2 * 4 : k2 * 4 + 4, :, 0:128].reshape(512, 128)
            vals = kv[p, k2 * 4 : k2 * 4 + 4, :, 128:384].reshape(512, 256)

            def rows(i, _):
                r = pl.ds(pl.multiple_of(i * 512, 512), 512)
                sc = lax.dot_general(
                    qp[p, r, :], keys, (((1,), (1,)), ((), ())), preferred_element_type=F32
                )
                top = jnp.max(sc, axis=1, keepdims=True)
                if not fresh:
                    old = mx[p, r, 0:1]
                    top = jnp.maximum(top, old)
                e = jnp.exp(sc - top).astype(BF16)
                o = jnp.dot(e, vals, preferred_element_type=F32)
                if not fresh:
                    o = o + acc[p, r, :] * jnp.exp(old - top)
                acc[p, r, :] = o
                mx[p, r, :] = jnp.broadcast_to(top, (512, 128))
                return 0

            lax.fori_loop(0, 2, rows, 0)

    stripe(0, True)
    for k1 in (0, 1, 2, 3):
        k2 = 1 if k1 < 2 else 3
        for p in range(2):
            gather_second(p, k2, k1).wait_recv()
            gather_second(p, 2, k1).start()
    for k2, rest in ((1, (2, 3)), (3, (0, 1))):
        for k1 in rest:
            for p in range(2):
                gather_second(p, k2, k1).wait_recv()
        stripe(k2, False)
    for k1 in range(4):
        for p in range(2):
            gather_second(p, 2, k1).wait_recv()
    stripe(2, False)

    for b in range(8):
        p, pos, i = b // 4, (b // 2) % 2, (b % 4) * 2
        o = []
        for j in (i, i + 1):
            r = slice(j * 128, (j + 1) * 128)
            o.append(acc[p, r, 0:128] / acc[p, r, 128:256])
        if pos == 0:
            a = jnp.where(low, o[0], pltpu.roll(o[1], 64, 1))
        else:
            a = jnp.where(low, pltpu.roll(o[0], 64, 1), o[1])
        att[:, b * 128 : (b + 1) * 128] = a.astype(BF16)

    weights[0].wait()
    projected = jnp.dot(att[...], wo[...], preferred_element_type=F32)
    fr = (res_ref[0].astype(F32) + rms(projected) * mix_ref[...]).astype(BF16)
    first[...] = fr
    normed[...] = (rms(fr.astype(F32)) * ffn_ref[...]).astype(BF16)

    def cols_of(p):
        return pl.ds(PARTS[p][1], PARTS[p][2])

    def canon(p, k2, k1, k3, kc):
        rel = dict(zip(PARTS[p][0], (k1, k2, k3)))
        return rel[1], rel[0], (rel[2] * 2 + kc) * 4

    def remote(src, dst, ss, rs, device):
        return pltpu.make_async_remote_copy(
            src_ref=src, dst_ref=dst, send_sem=ss, recv_sem=rs, device_id=device, device_id_type=MESH
        )

    def stage1(p, k1, back):
        axis = PARTS[p][0][0]
        c = cols_of(p)
        if back:
            return remote(inboxr.at[k1, :, c], outr.at[k1, :, c], r3s.at[p, k1], r3r.at[p, k1], dev(axis, 4 - k1))
        return remote(outbox.at[k1, :, c], inbox.at[k1, :, c], f1s.at[p, k1], f1r.at[p, k1], dev(axis, k1))

    def stage2(p, k2, k1, back):
        axis = PARTS[p][0][1]
        c = cols_of(p)
        if back:
            dst = (outr if k1 == 0 else inboxr).at[k1, pl.ds(k2 * 32, 32), c]
            return remote(midr.at[k2, k1, :, c], dst, r2s.at[p, k2, k1], r2r.at[p, k2, k1], dev(axis, 4 - k2))
        src = (outbox if k1 == 0 else inbox).at[k1, pl.ds(k2 * 32, 32), c]
        return remote(src, mid.at[k2, k1, :, c], f2s.at[p, k2, k1], f2r.at[p, k2, k1], dev(axis, k2))

    def hold(p, k2, k1, k3, kc, back):
        r = k3 * 8 + kc * 4
        c = cols_of(p)
        if k2 > 0:
            return (midr if back else mid).at[k2, k1, pl.ds(r, 4), c]
        if k1 > 0:
            return (inboxr if back else inbox).at[k1, pl.ds(r, 4), c]
        return (outr if back else outbox).at[0, pl.ds(r, 4), c]

    def stage3(p, k2, k1, k3, kc, back):
        axis = PARTS[p][0][2]
        ky, kz, r = canon(p, k2, k1, k3, kc)
        n = k3 * 2 + kc
        here = hold(p, k2, k1, k3, kc, back)
        c = cols_of(p)
        if n == 0:
            if back:
                return pltpu.make_async_copy(ys.at[ky, kz, pl.ds(r, 4), c], here, own_sem.at[1, p, k2, k1])
            return pltpu.make_async_copy(here, xs.at[ky, kz, pl.ds(r, 4), c], own_sem.at[0, p, k2, k1])
        if back:
            return remote(ys.at[ky, kz, pl.ds(r, 4), c], here, r1s.at[p, k2, k1, n], r1r.at[p, k2, k1, n], dev(axis, 4 - k3, kc))
        return remote(here, xs.at[ky, kz, pl.ds(r, 4), c], f3s.at[p, k2, k1, n], f3r.at[p, k2, k1, n], dev(axis, k3, kc))

    ALL3 = ((0, 0),) + tuple((k3, kc) for k3 in NEAR for kc in range(2)) + ((0, 1),)

    def fan(p, k2, k1):
        for k3, kc in ALL3:
            stage3(p, k2, k1, k3, kc, False).start()

    for p in range(3):
        c = slice(PARTS[p][1], PARTS[p][1] + PARTS[p][2])
        outbox[:, :, c] = (
            jnp.dot(disp[p], normed[:, c], preferred_element_type=F32)
            .astype(BF16)
            .reshape(4, 128, PARTS[p][2])
        )
        for k1 in NEAR:
            stage1(p, k1, False).start()
        for k2 in NEAR:
            stage2(p, k2, 0, False).start()
    for p in range(3):
        fan(p, 0, 0)
    for k1 in NEAR:
        for p in range(3):
            stage1(p, k1, False).wait_recv()
            for k2 in NEAR:
                stage2(p, k2, k1, False).start()
            fan(p, 0, k1)
    for k1 in (0,) + NEAR:
        for k2 in NEAR:
            for p in range(3):
                stage2(p, k2, k1, False).wait_recv()
                fan(p, k2, k1)

    weights[1].wait()
    weights[2].wait()
    for p in range(3):
        for k2 in range(4):
            for k1 in range(4):
                for k3 in range(4):
                    for kc in range(2):
                        cp = stage3(p, k2, k1, k3, kc, False)
                        if (k3, kc) == (0, 0):
                            cp.wait()
                        else:
                            cp.wait_recv()
        c = slice(PARTS[p][1], PARTS[p][1] + PARTS[p][2])

        def up(i, _):
            x = xs[i, :, :, c].reshape(128, PARTS[p][2])
            g = jnp.dot(x, wg[c, :], preferred_element_type=F32)
            u = jnp.dot(x, wu[c, :], preferred_element_type=F32)
            if p > 0:
                g, u = g + hg[i], u + hu[i]
            hg[i] = g
            hu[i] = u
            return 0

        lax.fori_loop(0, 4, up, 0)

    weights[3].wait()
    hidden = (jax.nn.silu(hg[...]) * hu[...]).astype(BF16).reshape(SLOTS, 512)
    for p in range(3):
        c = slice(PARTS[p][1], PARTS[p][1] + PARTS[p][2])
        ys[:, :, :, c] = (
            jnp.dot(hidden, wd[:, c], preferred_element_type=F32)
            .astype(BF16)
            .reshape(4, 4, 32, PARTS[p][2])
        )
        for k2 in NEAR + (0,):
            for k1 in NEAR + (0,):
                for k3, kc in ALL3:
                    stage3(p, k2, k1, k3, kc, True).start()

    def arrived3(p, k2, k1):
        for k3, kc in ALL3:
            cp = stage3(p, k2, k1, k3, kc, True)
            if (k3, kc) == (0, 0):
                cp.wait()
            else:
                cp.wait_recv()

    for k2 in NEAR:
        for k1 in NEAR + (0,):
            for p in range(3):
                arrived3(p, k2, k1)
                stage2(p, k2, k1, True).start()
    for k1 in NEAR:
        for p in range(3):
            arrived3(p, 0, k1)
            for k2 in NEAR:
                stage2(p, k2, k1, True).wait_recv()
            stage1(p, k1, True).start()
    for p in range(3):
        arrived3(p, 0, 0)
        for k2 in NEAR:
            stage2(p, k2, 0, True).wait_recv()

    g0, g1 = gate_ref[0, :, 0:1], gate_ref[0, :, 1:2]
    sums = []
    for p in range(3):
        for k1 in NEAR:
            stage1(p, k1, True).wait_recv()
        c = slice(PARTS[p][1], PARTS[p][1] + PARTS[p][2])
        back = outr[:, :, c].reshape(SLOTS, PARTS[p][2])
        a0 = jnp.dot(comb[p, 0], back, preferred_element_type=F32)
        a1 = jnp.dot(comb[p, 1], back, preferred_element_type=F32)
        sums.append(g0 * a0 + g1 * a1)
    total = jnp.concatenate(sums, axis=1)
    out_ref[0] = (first[...].astype(F32) + rms(total) * post_ref[...]).astype(BF16)

    for p in range(2):
        for k1 in NEAR:
            gather_first(p, k1).wait_send()
        for k2 in NEAR:
            for k1 in range(4):
                gather_second(p, k2, k1).wait_send()
    for p in range(3):
        for back in (False, True):
            for k1 in NEAR:
                stage1(p, k1, back).wait_send()
            for k2 in NEAR:
                for k1 in range(4):
                    stage2(p, k2, k1, back).wait_send()
            for k2 in range(4):
                for k1 in range(4):
                    for k3, kc in SIDES:
                        stage3(p, k2, k1, k3, kc, back).wait_send()


def shards(
    queries, keys, values, q_gain, k_gain, residual, out_weight, mix_gain, ffn_gain, post_gain,
    expert_ids, expert_gate, w_gate, w_up, w_down,
):
    rows, cols = tables()
    vm = pl.BlockSpec(memory_space=pltpu.VMEM)
    hbm = pl.BlockSpec(memory_space=pl.ANY)
    sem = pltpu.SemaphoreType.DMA
    box = pltpu.VMEM((4, 128, D), BF16)
    deep = pltpu.VMEM((4, 4, 32, D), BF16)
    return pl.pallas_call(
        kernel,
        out_shape=jax.ShapeDtypeStruct((1, TOK, D), BF16),
        in_specs=[vm, vm, vm, vm, vm, vm, hbm, vm, vm, vm, vm, vm, hbm, hbm, hbm, vm, vm],
        out_specs=vm,
        scratch_shapes=[
            pltpu.VMEM((1024, D), BF16),
            pltpu.VMEM((D, 512), BF16),
            pltpu.VMEM((D, 512), BF16),
            pltpu.VMEM((512, D), BF16),
            pltpu.VMEM((2, 1024, 128), BF16),
            pltpu.VMEM((2, 16, TOK, 384), BF16),
            pltpu.VMEM((2, 1024, 128), F32),
            pltpu.VMEM((2, 1024, 256), F32),
            pltpu.VMEM((TOK, 1024), BF16),
            pltpu.VMEM((TOK, D), BF16),
            pltpu.VMEM((TOK, D), BF16),
            pltpu.VMEM((3, SLOTS, 128), BF16),
            pltpu.VMEM((3, 2, 128, SLOTS), BF16),
            box, box, deep, deep, deep, deep, box, box,
            pltpu.VMEM((4, 128, 512), F32),
            pltpu.VMEM((4, 128, 512), F32),
            sem((4,)),
            sem((2, 16)), sem((2, 16)),
            sem((3, 4)), sem((3, 4)),
            sem((3, 4, 4)), sem((3, 4, 4)),
            sem((3, 4, 4, 8)), sem((3, 4, 4, 8)),
            sem((3, 4, 4, 8)), sem((3, 4, 4, 8)),
            sem((3, 4, 4)), sem((3, 4, 4)),
            sem((3, 4)), sem((3, 4)),
            sem((2, 3, 4, 4)),
        ],
        compiler_params=pltpu.CompilerParams(
            collective_id=0, has_side_effects=True, vmem_limit_bytes=60 * 2**20
        ),
        name="layer",
    )(
        queries, keys, values, q_gain[None], k_gain[None], residual, out_weight,
        mix_gain[None], ffn_gain[None], post_gain[None], expert_ids, expert_gate,
        w_gate, w_up, w_down, jnp.asarray(rows), jnp.asarray(cols),
    )


def solution(mesh):
    return jax.shard_map(
        shards,
        mesh=mesh,
        in_specs=(
            P("dp", "sp", None), P("dp", "sp", None), P("dp", "sp", None), P(), P(),
            P("dp", "sp", None), P(), P(), P(), P(),
            P("dp", "sp", None), P("dp", "sp", None),
            P(("sp", "dp"), None, None), P(("sp", "dp"), None, None), P(("sp", "dp"), None, None),
        ),
        out_specs=P("dp", "sp", None),
        check_vma=False,
    )
```

time: 209 us -> 121 us (0.58)
  Pallas kernels: 0 us -> 116 us
  waiting for transfers between devices: 47.9 us -> 0 us
  local copies, waits for them, and re-layouts: 50.5 us -> 4.7 us
  blocking collectives: 36.6 us -> 0 us
  starting transfers between devices: 26.9 us -> 0 us
  matrix products: 21.8 us -> 0 us
  other arithmetic: 15.3 us -> 0 us
  loops' own time: 7.87 us -> 0 us
    pallas_call x0 -> x1, Pallas kernels: none -> 116 us  [shards(): pl.pallas_call(kernel, out_shape=jax.ShapeDtypeStruct((1, TOK, D), BF16),...]
    all_to_all x5 -> x0, waiting for transfers between devices: 47.9 us -> none  [the longest x1 29.6 us: shards(): lax.all_to_all(answer.reshape(layout), ('sp', 'dp'), split_axis=0, concat...]
    all_to_all x1 -> x0, blocking collectives: 36.6 us -> none  [shards(): lax.all_to_all(outbox, ('sp', 'dp'), split_axis=0, concat_axis=0, tiled=T...]
    all_to_all x5 -> x0, starting transfers between devices: 26.9 us -> none  [the longest x1 8.17 us: shards(): lax.all_to_all(key_rows, 'sp', split_axis=1, concat_axis=0, tiled=True)]
    dot_general x11 -> x0, matrix products: 21.8 us -> none  [the longest x1 6.22 us: shards(): jnp.dot(hidden, w_down[0], preferred_element_type=jnp.float32)]
    reshape x6 -> x0, local copies, waits for them, and re-layouts: 18.5 us -> none  [the longest x1 4.12 us: shards(): outbox = outbox.reshape(experts_all, capacity, D)]
    convert_element_type x7 -> x0, local copies, waits for them, and re-layouts: 9.2 us -> none  [the longest x4 5.61 us: rotate(): values = rms_scale(field.astype(jnp.float32)) * gain]
    reduce_sum x10 -> x0, other arithmetic: 8.96 us -> none  [the longest x1 4.81 us: shards(): expert_sum = jnp.sum(answers * expert_gate[0][:, :, None], axis=1)]
  transfers between devices with their start and end apart: 5 -> 0, of which waited for: 5 -> 0; matrix products, arithmetic and copies ran while one was open for 8% -> 0% of each run, Pallas kernels for 0% -> 0%
where the time goes in v1:
time: 121 us
  Pallas kernels  116 us (96%)
  local copies, waits for them, and re-layouts  4.7 us (4%)
    pallas_call x1, Pallas kernels, shards(): pl.pallas_call(kernel, out_shape=jax.ShapeDtypeStruct((1, TOK, D), BF16),...  116 us
    unnamed x3, local copies, waits for them, and re-layouts  4.7 us

profile of v1, /device:TPU:0, one launch (start us, length us, event | category | flops | bytes accessed | tf_op | source)
XLA Modules:
  0.0 121.0 jit_solution(14784306967451805205)
XLA Ops:
  0.0 1.4 %copy.18.ids_ref = s32[1,128,2]{2,1,0:T(8,128)} copy(s32[1,128,2]{1,2,0:T(2,128)} %param.27) | data formatting | bytes 2048 | tf_op args[10]
  1.4 1.4 %copy.19.gate_ref = f32[1,128,2]{2,1,0:T(8,128)} copy(f32[1,128,2]{1,2,0:T(2,128)} %param.28) | data formatting | bytes 2048 | tf_op args[11]
  2.8 116.3 %layer.1 = bf16[1,128,2048]{2,1,0:T(8,128)(2,1)} custom-call(bf16[1,128,1024]{2,1,0:T(8,128)(2,1)} %q_ref.1, bf16[1,128,256]{2,1,0:T(8,128)(2,1)} %k_ref.1, bf16[1,128,256]{2,1,0:T(8,128)(2,1)} %v_ref.1, f32[1,64]{1,0:T(1,128)} %bitcast.8, f32[1,64]{1,0:T(1,128)} %bitcast.9, bf16[1,128,2048]{2,1,0:T(8,128)(2,1)} %res_ref.1, bf16[1024,2048]{1,0:T(8,128)(2,1)} %wo_hbm.1, ...), custom_call_target="tpu_custom_call" | custom-call | tf_op jit(solution)/shard_map/layer/pallas_call | solution.py:428
  119.1 1.9 %copy.21 = bf16[1,128,2048]{2,1,0:T(8,128)(2,1)} copy(bf16[1,128,2048]{2,1,0:T(8,128)(2,1)} %layer.1) | data formatting | bytes 1048576

commit v2 on v1

--- a/solution.py
+++ b/solution.py
@@ -15,11 +15,17 @@
 D = 2048
 TOK = 128
 SLOTS = 512
-
-PARTS = (((0, 1, 2), 0, 640), ((1, 2, 0), 640, 640), ((2, 0, 1), 1280, 768))
+ROWS = 256
+
+PARTS = (
+    ((0, 1, 2), 0, 384), ((1, 2, 0), 384, 384), ((2, 0, 1), 768, 384),
+    ((0, 1, 2), 1152, 256), ((1, 2, 0), 1408, 256), ((2, 0, 1), 1664, 384),
+)
+WAVES = ((0, 1, 2), (3, 4, 5))
+NP = len(PARTS)
+PLACE = {0: 0, 1: 1, 3: 2, 2: 3}
 PAIRS = ((0, 1), (1, 0))
-NEAR = (1, 3, 2)
-SIDES = tuple((k3, kc) for k3 in range(4) for kc in range(2) if (k3, kc) != (0, 0))
+NEAR = (2, 1, 3)
 
 
 def tables():
@@ -51,7 +57,7 @@
     out_ref,
     wo, wg, wu, wd, qp, kv, mx, acc, att, first, normed, disp, comb,
     outbox, inbox, mid, xs, ys, midr, inboxr, outr, hg, hu,
-    wsem, gs, gr, f1s, f1r, f2s, f2r, f3s, f3r, r1s, r1r, r2s, r2r, r3s, r3r, own_sem,
+    wsem, gs, gr, f1r, f2r, f3r, r1r, r2r, r3r, sent,
 ):
     s = lax.axis_index("sp")
     d = lax.axis_index("dp")
@@ -110,34 +116,6 @@
         kv[p, 0, :, 128:256] = v_ref[0, :, cols]
         kv[p, :, :, 256:384] = jnp.ones((16, TOK, 128), BF16)
 
-    pl.semaphore_wait(barrier, len(peers))
-
-    def hop(p, axis, k, src, dst):
-        return pltpu.make_async_remote_copy(
-            src_ref=kv.at[p, src, :, pl.ds(0, 256)],
-            dst_ref=kv.at[p, dst, :, pl.ds(0, 256)],
-            send_sem=gs.at[p, dst],
-            recv_sem=gr.at[p, dst],
-            device_id=dev(axis, k),
-            device_id_type=MESH,
-        )
-
-    def gather_first(p, k1):
-        return hop(p, PAIRS[p][0], k1, 0, k1)
-
-    def gather_second(p, k2, k1):
-        if k2 == 2:
-            k = 1 if k1 < 2 else 3
-            return hop(p, PAIRS[p][1], k, k * 4 + k1, 8 + k1)
-        return hop(p, PAIRS[p][1], k2, k1, k2 * 4 + k1)
-
-    for k1 in NEAR:
-        for p in range(2):
-            gather_first(p, k1).start()
-    for k2 in (1, 3):
-        for p in range(2):
-            gather_second(p, k2, 0).start()
-
     for b in range(8):
         t = turn(q_ref[0, :, b * 128 : (b + 1) * 128], qgain).astype(BF16).astype(F32) * 0.125
         flip = pltpu.roll(t, 64, 1)
@@ -149,6 +127,34 @@
         qp[p, i * 128 : (i + 1) * 128] = a0.astype(BF16)
         qp[p, (i + 1) * 128 : (i + 2) * 128] = a1.astype(BF16)
 
+    pl.semaphore_wait(barrier, len(peers))
+
+    def hop(p, axis, k, src, dst):
+        return pltpu.make_async_remote_copy(
+            src_ref=kv.at[p, src, :, pl.ds(0, 256)],
+            dst_ref=kv.at[p, dst, :, pl.ds(0, 256)],
+            send_sem=gs.at[p, dst // 4],
+            recv_sem=gr.at[p, dst],
+            device_id=dev(axis, k),
+            device_id_type=MESH,
+        )
+
+    def gather_first(p, k1):
+        return hop(p, PAIRS[p][0], k1, 0, k1)
+
+    def gather_second(p, k2, k1):
+        if k2 == 2:
+            k = 1 if k1 < 2 else 3
+            return hop(p, PAIRS[p][1], k, PLACE[k] * 4 + k1, PLACE[2] * 4 + k1)
+        return hop(p, PAIRS[p][1], k2, k1, PLACE[k2] * 4 + k1)
+
+    for k1 in NEAR:
+        for p in range(2):
+            gather_first(p, k1).start()
+    for k2 in (1, 3):
+        for p in range(2):
+            gather_second(p, k2, 0).start()
+
     for k1 in NEAR:
         for p in range(2):
             gather_first(p, k1).wait_recv()
@@ -158,18 +164,17 @@
     tok_r = lax.broadcasted_iota(jnp.int32, (128, 128), 0)
     tok_c = lax.broadcasted_iota(jnp.int32, (128, 128), 1)
     before = (tok_r < tok_c).astype(F32).astype(BF16)
-    ids = ids_ref[0].astype(F32)
-    idt = [jnp.transpose(jnp.broadcast_to(ids[:, k : k + 1], (128, 128))) for k in range(2)]
-    hot = [(t == tok_r.astype(F32)).astype(F32) for t in idt]
+    idt = [ids_ref[k : k + 1, :] for k in range(2)]
+    hot = [(t == tok_r).astype(F32) for t in idt]
     cnt = [jnp.dot(h.astype(BF16), before, preferred_element_type=F32) for h in hot]
     cnt[1] = cnt[1] + jnp.sum(hot[0], axis=1, keepdims=True)
     rank = [jnp.sum(h * c, axis=0, keepdims=True).astype(jnp.int32) for h, c in zip(hot, cnt)]
     slot_row = lax.broadcasted_iota(jnp.int32, (SLOTS, 128), 0)
     slot_col = lax.broadcasted_iota(jnp.int32, (128, SLOTS), 1).astype(F32)
-    for p, (axes, _, _) in enumerate(PARTS):
+    for p, (axes, _, _) in enumerate(PARTS[:3]):
         slots = []
         for k in range(2):
-            e = idt[k][0:1].astype(jnp.int32)
+            e = idt[k]
             at = (e // 32, (e // 8) % 4, (e // 2) % 4)
             rel = [(at[a] - mine[a] + 4) % 4 for a in axes]
             kc = (e % 2 + core) % 2
@@ -179,31 +184,30 @@
             col = jnp.transpose(jnp.broadcast_to(slots[k].astype(F32), (128, 128)))[:, 0:1]
             comb[p, k] = (slot_col == col).astype(F32).astype(BF16)
 
-    def stripe(k2, fresh):
-        for p in range(2):
-            keys = kv[p, k2 * 4 : k2 * 4 + 4, :, 0:128].reshape(512, 128)
-            vals = kv[p, k2 * 4 : k2 * 4 + 4, :, 128:384].reshape(512, 256)
-
-            def rows(i, _):
-                r = pl.ds(pl.multiple_of(i * 512, 512), 512)
+    def stripe(first_place, count, fresh):
+        for p in range(2):
+            span = slice(first_place * 4, (first_place + count) * 4)
+            n = count * 512
+            keys = kv[p, span, :, 0:128].reshape(n, 128)
+            vals = kv[p, span, :, 128:384].reshape(n, 256)
+            for i in range(1024 // ROWS):
+                r = slice(i * ROWS, (i + 1) * ROWS)
                 sc = lax.dot_general(
                     qp[p, r, :], keys, (((1,), (1,)), ((), ())), preferred_element_type=F32
                 )
-                top = jnp.max(sc, axis=1, keepdims=True)
+                top = jnp.broadcast_to(jnp.max(sc, axis=1, keepdims=True), (ROWS, 128))
                 if not fresh:
-                    old = mx[p, r, 0:1]
+                    old = mx[p, r, :]
                     top = jnp.maximum(top, old)
-                e = jnp.exp(sc - top).astype(BF16)
+                    fade = jnp.exp(old - top)
+                mx[p, r, :] = top
+                e = jnp.exp(sc - jnp.concatenate([top] * (n // 128), axis=1)).astype(BF16)
                 o = jnp.dot(e, vals, preferred_element_type=F32)
                 if not fresh:
-                    o = o + acc[p, r, :] * jnp.exp(old - top)
+                    o = o + acc[p, r, :] * jnp.concatenate([fade, fade], axis=1)
                 acc[p, r, :] = o
-                mx[p, r, :] = jnp.broadcast_to(top, (512, 128))
-                return 0
-
-            lax.fori_loop(0, 2, rows, 0)
-
-    stripe(0, True)
+
+    stripe(0, 1, True)
     for k1 in (0, 1, 2, 3):
         k2 = 1 if k1 < 2 else 3
         for p in range(2):
@@ -213,11 +217,11 @@
         for k1 in rest:
             for p in range(2):
                 gather_second(p, k2, k1).wait_recv()
-        stripe(k2, False)
+    stripe(1, 2, False)
     for k1 in range(4):
         for p in range(2):
             gather_second(p, 2, k1).wait_recv()
-    stripe(2, False)
+    stripe(3, 1, False)
 
     for b in range(8):
         p, pos, i = b // 4, (b // 2) % 2, (b % 4) * 2
@@ -253,17 +257,17 @@
         axis = PARTS[p][0][0]
         c = cols_of(p)
         if back:
-            return remote(inboxr.at[k1, :, c], outr.at[k1, :, c], r3s.at[p, k1], r3r.at[p, k1], dev(axis, 4 - k1))
-        return remote(outbox.at[k1, :, c], inbox.at[k1, :, c], f1s.at[p, k1], f1r.at[p, k1], dev(axis, k1))
+            return remote(inboxr.at[k1, :, c], outr.at[k1, :, c], sent.at[p, 5], r3r.at[p], dev(axis, 4 - k1))
+        return remote(outbox.at[k1, :, c], inbox.at[k1, :, c], sent.at[p, 0], f1r.at[p, k1 - 1], dev(axis, k1))
 
     def stage2(p, k2, k1, back):
         axis = PARTS[p][0][1]
         c = cols_of(p)
         if back:
             dst = (outr if k1 == 0 else inboxr).at[k1, pl.ds(k2 * 32, 32), c]
-            return remote(midr.at[k2, k1, :, c], dst, r2s.at[p, k2, k1], r2r.at[p, k2, k1], dev(axis, 4 - k2))
+            return remote(midr.at[k2, k1, :, c], dst, sent.at[p, 4], r2r.at[p, k1], dev(axis, 4 - k2))
         src = (outbox if k1 == 0 else inbox).at[k1, pl.ds(k2 * 32, 32), c]
-        return remote(src, mid.at[k2, k1, :, c], f2s.at[p, k2, k1], f2r.at[p, k2, k1], dev(axis, k2))
+        return remote(src, mid.at[k2, k1, :, c], sent.at[p, 1], f2r.at[p, k1], dev(axis, k2))
 
     def hold(p, k2, k1, k3, kc, back):
         r = k3 * 8 + kc * 4
@@ -280,13 +284,17 @@
         n = k3 * 2 + kc
         here = hold(p, k2, k1, k3, kc, back)
         c = cols_of(p)
+        far = xs.at[ky, kz, pl.ds(r, 4), c] if not back else ys.at[ky, kz, pl.ds(r, 4), c]
         if n == 0:
             if back:
-                return pltpu.make_async_copy(ys.at[ky, kz, pl.ds(r, 4), c], here, own_sem.at[1, p, k2, k1])
-            return pltpu.make_async_copy(here, xs.at[ky, kz, pl.ds(r, 4), c], own_sem.at[0, p, k2, k1])
+                return pltpu.make_async_copy(far, here, r1r.at[p, k2])
+            return pltpu.make_async_copy(here, far, f3r.at[p])
         if back:
-            return remote(ys.at[ky, kz, pl.ds(r, 4), c], here, r1s.at[p, k2, k1, n], r1r.at[p, k2, k1, n], dev(axis, 4 - k3, kc))
-        return remote(here, xs.at[ky, kz, pl.ds(r, 4), c], f3s.at[p, k2, k1, n], f3r.at[p, k2, k1, n], dev(axis, k3, kc))
+            return remote(far, here, sent.at[p, 3], r1r.at[p, k2], dev(axis, 4 - k3, kc))
+        return remote(here, far, sent.at[p, 2], f3r.at[p], dev(axis, k3, kc))
+
+    def drain(ref, sem):
+        pltpu.make_async_copy(ref, ref, sem).wait()
 
     ALL3 = ((0, 0),) + tuple((k3, kc) for k3 in NEAR for kc in range(2)) + ((0, 1),)
 
@@ -294,10 +302,10 @@
         for k3, kc in ALL3:
             stage3(p, k2, k1, k3, kc, False).start()
 
-    for p in range(3):
+    for p in range(NP):
         c = slice(PARTS[p][1], PARTS[p][1] + PARTS[p][2])
         outbox[:, :, c] = (
-            jnp.dot(disp[p], normed[:, c], preferred_element_type=F32)
+            jnp.dot(disp[p % 3], normed[:, c], preferred_element_type=F32)
             .astype(BF16)
             .reshape(4, 128, PARTS[p][2])
         )
@@ -305,32 +313,26 @@
             stage1(p, k1, False).start()
         for k2 in NEAR:
             stage2(p, k2, 0, False).start()
-    for p in range(3):
+    for p in range(NP):
         fan(p, 0, 0)
-    for k1 in NEAR:
-        for p in range(3):
-            stage1(p, k1, False).wait_recv()
-            for k2 in NEAR:
-                stage2(p, k2, k1, False).start()
-            fan(p, 0, k1)
-    for k1 in (0,) + NEAR:
-        for k2 in NEAR:
-            for p in range(3):
-                stage2(p, k2, k1, False).wait_recv()
-                fan(p, k2, k1)
+    for wave in WAVES:
+        for k1 in (1, 3, 2):
+            for p in wave:
+                drain(inbox.at[k1, :, cols_of(p)], f1r.at[p, k1 - 1])
+                for k2 in NEAR:
+                    stage2(p, k2, k1, False).start()
+                fan(p, 0, k1)
+    for wave in WAVES:
+        for k1 in (0, 1, 3, 2):
+            for p in wave:
+                drain(mid.at[pl.ds(1, 3), k1, :, cols_of(p)], f2r.at[p, k1])
+                for k2 in NEAR:
+                    fan(p, k2, k1)
 
     weights[1].wait()
     weights[2].wait()
-    for p in range(3):
-        for k2 in range(4):
-            for k1 in range(4):
-                for k3 in range(4):
-                    for kc in range(2):
-                        cp = stage3(p, k2, k1, k3, kc, False)
-                        if (k3, kc) == (0, 0):
-                            cp.wait()
-                        else:
-                            cp.wait_recv()
+    for p in range(NP):
+        drain(xs.at[:, :, :, cols_of(p)], f3r.at[p])
         c = slice(PARTS[p][1], PARTS[p][1] + PARTS[p][2])
 
         def up(i, _):
@@ -347,7 +349,7 @@
 
     weights[3].wait()
     hidden = (jax.nn.silu(hg[...]) * hu[...]).astype(BF16).reshape(SLOTS, 512)
-    for p in range(3):
+    for p in range(NP):
         c = slice(PARTS[p][1], PARTS[p][1] + PARTS[p][2])
         ys[:, :, :, c] = (
             jnp.dot(hidden, wd[:, c], preferred_element_type=F32)
@@ -359,60 +361,45 @@
                 for k3, kc in ALL3:
                     stage3(p, k2, k1, k3, kc, True).start()
 
-    def arrived3(p, k2, k1):
-        for k3, kc in ALL3:
-            cp = stage3(p, k2, k1, k3, kc, True)
-            if (k3, kc) == (0, 0):
-                cp.wait()
-            else:
-                cp.wait_recv()
-
-    for k2 in NEAR:
-        for k1 in NEAR + (0,):
-            for p in range(3):
-                arrived3(p, k2, k1)
-                stage2(p, k2, k1, True).start()
-    for k1 in NEAR:
-        for p in range(3):
-            arrived3(p, 0, k1)
-            for k2 in NEAR:
-                stage2(p, k2, k1, True).wait_recv()
-            stage1(p, k1, True).start()
-    for p in range(3):
-        arrived3(p, 0, 0)
+    for wave in WAVES:
         for k2 in NEAR:
-            stage2(p, k2, 0, True).wait_recv()
-
-    g0, g1 = gate_ref[0, :, 0:1], gate_ref[0, :, 1:2]
+            for p in wave:
+                drain(midr.at[k2, :, :, cols_of(p)], r1r.at[p, k2])
+                for k1 in (2, 1, 3, 0):
+                    stage2(p, k2, k1, True).start()
+        for p in wave:
+            drain(midr.at[0, :, :, cols_of(p)], r1r.at[p, 0])
+    for wave in WAVES:
+        for k1 in NEAR:
+            for p in wave:
+                drain(inboxr.at[k1, pl.ds(32, 96), cols_of(p)], r2r.at[p, k1])
+                stage1(p, k1, True).start()
+        for p in wave:
+            drain(outr.at[0, pl.ds(32, 96), cols_of(p)], r2r.at[p, 0])
+
+    g0, g1 = [jnp.transpose(jnp.broadcast_to(gate_ref[k : k + 1, :], (128, 128))) for k in range(2)]
     sums = []
-    for p in range(3):
-        for k1 in NEAR:
-            stage1(p, k1, True).wait_recv()
+    for p in range(NP):
+        drain(outr.at[pl.ds(1, 3), :, cols_of(p)], r3r.at[p])
         c = slice(PARTS[p][1], PARTS[p][1] + PARTS[p][2])
         back = outr[:, :, c].reshape(SLOTS, PARTS[p][2])
-        a0 = jnp.dot(comb[p, 0], back, preferred_element_type=F32)
-        a1 = jnp.dot(comb[p, 1], back, preferred_element_type=F32)
-        sums.append(g0 * a0 + g1 * a1)
+        a0 = jnp.dot(comb[p % 3, 0], back, preferred_element_type=F32)
+        a1 = jnp.dot(comb[p % 3, 1], back, preferred_element_type=F32)
+        wide = PARTS[p][2] // 128
+        sums.append(jnp.concatenate([g0] * wide, axis=1) * a0 + jnp.concatenate([g1] * wide, axis=1) * a1)
     total = jnp.concatenate(sums, axis=1)
     out_ref[0] = (first[...].astype(F32) + rms(total) * post_ref[...]).astype(BF16)
 
     for p in range(2):
-        for k1 in NEAR:
-            gather_first(p, k1).wait_send()
-        for k2 in NEAR:
-            for k1 in range(4):
-                gather_second(p, k2, k1).wait_send()
-    for p in range(3):
-        for back in (False, True):
-            for k1 in NEAR:
-                stage1(p, k1, back).wait_send()
-            for k2 in NEAR:
-                for k1 in range(4):
-                    stage2(p, k2, k1, back).wait_send()
-            for k2 in range(4):
-                for k1 in range(4):
-                    for k3, kc in SIDES:
-                        stage3(p, k2, k1, k3, kc, back).wait_send()
+        drain(kv.at[p, pl.ds(0, 3), :, pl.ds(0, 256)], gs.at[p, 0])
+        for i in range(1, 4):
+            drain(kv.at[p, pl.ds(0, 4), :, pl.ds(0, 256)], gs.at[p, i])
+    for p in range(NP):
+        c = cols_of(p)
+        for i in (0, 1, 4, 5):
+            drain(outbox.at[pl.ds(1, 3), :, c], sent.at[p, i])
+        for i in (2, 3):
+            drain(outbox.at[:, pl.ds(0, 112), c], sent.at[p, i])
 
 
 def shards(
@@ -448,14 +435,10 @@
             pltpu.VMEM((4, 128, 512), F32),
             pltpu.VMEM((4, 128, 512), F32),
             sem((4,)),
-            sem((2, 16)), sem((2, 16)),
-            sem((3, 4)), sem((3, 4)),
-            sem((3, 4, 4)), sem((3, 4, 4)),
-            sem((3, 4, 4, 8)), sem((3, 4, 4, 8)),
-            sem((3, 4, 4, 8)), sem((3, 4, 4, 8)),
-            sem((3, 4, 4)), sem((3, 4, 4)),
-            sem((3, 4)), sem((3, 4)),
-            sem((2, 3, 4, 4)),
+            sem((2, 4)), sem((2, 16)),
+            sem((NP, 3)), sem((NP, 4)), sem((NP,)),
+            sem((NP, 4)), sem((NP, 4)), sem((NP,)),
+            sem((NP, 6)),
         ],
         compiler_params=pltpu.CompilerParams(
             collective_id=0, has_side_effects=True, vmem_limit_bytes=60 * 2**20
@@ -463,7 +446,7 @@
         name="layer",
     )(
         queries, keys, values, q_gain[None], k_gain[None], residual, out_weight,
-        mix_gain[None], ffn_gain[None], post_gain[None], expert_ids, expert_gate,
+        mix_gain[None], ffn_gain[None], post_gain[None], expert_ids[0].T, expert_gate[0].T,
         w_gate, w_up, w_down, jnp.asarray(rows), jnp.asarray(cols),
     )
 

time: 121 us -> 89.5 us (0.74)
  Pallas kernels: 116 us -> 86.7 us
  local copies, waits for them, and re-layouts: 4.7 us -> 1.88 us
    pallas_call x1, Pallas kernels: 116 us -> 86.7 us  [shards(): pl.pallas_call(kernel, out_shape=jax.ShapeDtypeStruct((1, TOK, D), BF16),...]
    unnamed x3 -> x1, local copies, waits for them, and re-layouts: 4.7 us -> 1.88 us
where the time goes in v2:
time: 89.5 us; the launch traced here: 88.6 us
  Pallas kernels  86.7 us (97%)
  local copies, waits for them, and re-layouts  1.88 us (2%)
    pallas_call x1, Pallas kernels, shards(): pl.pallas_call(kernel, out_shape=jax.ShapeDtypeStruct((1, TOK, D), BF16),...  86.7 us
    unnamed x1, local copies, waits for them, and re-layouts  1.88 us

profile of v2, /device:TPU:0, one launch (start us, length us, event | category | flops | bytes accessed | tf_op | source)
XLA Modules:
  0.0 88.6 jit_solution(6400148999093559129)
XLA Ops:
  0.0 86.7 %layer.1 = bf16[1,128,2048]{2,1,0:T(8,128)(2,1)} custom-call(bf16[1,128,1024]{2,1,0:T(8,128)(2,1)} %q_ref.1, bf16[1,128,256]{2,1,0:T(8,128)(2,1)} %k_ref.1, bf16[1,128,256]{2,1,0:T(8,128)(2,1)} %v_ref.1, f32[1,64]{1,0:T(1,128)} %bitcast.16, f32[1,64]{1,0:T(1,128)} %bitcast.17, bf16[1,128,2048]{2,1,0:T(8,128)(2,1)} %res_ref.1, bf16[1024,2048]{1,0:T(8,128)(2,1)} %wo_hbm.1, ...), custom_call_target="tpu_custom_call" | custom-call | tf_op jit(solution)/shard_map/layer/pallas_call | solution.py:415
  86.7 1.9 %copy.19 = bf16[1,128,2048]{2,1,0:T(8,128)(2,1)} copy(bf16[1,128,2048]{2,1,0:T(8,128)(2,1)} %layer.1) | data formatting | bytes 1048576

commit v3 on v2

v3 whole, which is shorter than its diff:
```python
import functools

import numpy as np
import jax
import jax.numpy as jnp
from jax import lax
from jax.experimental import pallas as pl
from jax.experimental.pallas import tpu as pltpu
from jax.sharding import PartitionSpec as P

MESH = pl.DeviceIdType.MESH
F32, BF16 = jnp.float32, jnp.bfloat16
EPS = 1e-06
GRID = 64
D = 2048
TOK = 128
SLOTS = 512
ROWS = 256
LIMIT = 60 * 2**20

PARTS = (((0, 1, 2), 0, 640), ((1, 2, 0), 640, 640), ((2, 0, 1), 1280, 768))
UNITS = tuple((w, p) for w in range(2) for p in range(3))
PLACE = {0: 0, 1: 1, 3: 2, 2: 3}
PAIRS = ((0, 1), (1, 0))
NEAR = (2, 1, 3)


def tables():
    lane = np.arange(128) % 64
    pair = lane // 2
    freq = 10000.0 ** (-4.0 * (pair % 16) / 64.0)
    sign = np.where(lane % 2 == 0, -1.0, 1.0)
    row_lane = pair < 16
    rows = np.zeros((16, 8, 128), np.float32)
    for s in range(16):
        for i in range(2):
            ang = (2 * s + i) * freq
            rows[s, i] = np.where(row_lane, np.cos(ang), 0.0)
            rows[s, 2 + i] = np.where(row_lane, np.sin(ang) * sign, 0.0)
    ang = np.arange(64)[:, None] * freq[None, :]
    cols = np.stack(
        [np.where(row_lane, 0.0, np.cos(ang)), np.where(row_lane, 0.0, np.sin(ang) * sign)]
    ).astype(np.float32)
    return rows, cols


def rms(v):
    return v * lax.rsqrt(jnp.mean(v * v, axis=-1, keepdims=True) + EPS)


def kernel(
    k_hbm, v_hbm, kg_hbm, rtab_hbm, ctab_hbm, q_hbm, qg_hbm, ids_hbm, gate_hbm, res_hbm,
    mix_hbm, ffn_hbm, post_hbm, wo_hbm, wg_hbm, wu_hbm, wd_hbm,
    out_ref,
    k_ref, v_ref, kg_ref, rtab_ref, ctab_ref, q_ref, qg_ref, ids_ref, gate_ref, res_ref,
    mix_ref, ffn_ref, post_ref,
    wo, wg, wu, wd, qp, kv, mx, acc, att, first, normed, disp, comb,
    outbox, inbox, mid, xs, ys, midr, inboxr, outr, tot,
    wsem, gs, gr, f1r, f2r, f3r, r1r, r1z, r2r, r3r, sent,
):
    s = lax.axis_index("sp")
    d = lax.axis_index("dp")
    mine = (s // 4, s % 4, d // 2)
    core = d % 2

    def dev(axis, k, kc=0):
        p = list(mine)
        p[axis] = (p[axis] + k) % 4
        return (p[0] * 4 + p[1], p[2] * 2 + (core + kc) % 2)

    def drain(ref, sem):
        pltpu.make_async_copy(ref, ref, sem).wait()

    barrier = pltpu.get_barrier_semaphore()
    peers = [dev(a, k, kc) for a in range(3) for k in NEAR for kc in range(2)] + [dev(0, 0, 1)]
    for peer in peers:
        pl.semaphore_signal(barrier, 1, device_id=peer, device_id_type=MESH)

    loads = [
        pltpu.make_async_copy(src, dst, wsem.at[i])
        for i, (src, dst) in enumerate(
            (
                (k_hbm, k_ref), (v_hbm, v_ref), (kg_hbm, kg_ref), (rtab_hbm, rtab_ref), (ctab_hbm, ctab_ref),
                (q_hbm, q_ref), (qg_hbm, qg_ref), (ids_hbm, ids_ref), (gate_hbm, gate_ref), (res_hbm, res_ref),
                (mix_hbm, mix_ref), (ffn_hbm, ffn_ref), (post_hbm, post_ref),
                (wo_hbm, wo), (wg_hbm.at[0], wg), (wu_hbm.at[0], wu), (wd_hbm.at[0], wd),
            )
        )
    ]
    for load in loads:
        load.start()

    def loaded(first_load, last_load):
        for load in loads[first_load:last_load]:
            load.wait()

    lane = lax.broadcasted_iota(jnp.int32, (TOK, 128), 1)
    even = (lane % 2) == 0
    low = lane < 64
    seg = jnp.where(
        (lax.broadcasted_iota(jnp.int32, (128, 128), 0) // 64)
        == (lax.broadcasted_iota(jnp.int32, (128, 128), 1) // 64),
        1.0 / 64.0,
        0.0,
    ).astype(BF16)
    loaded(0, 5)
    rt = rtab_ref[s]
    cos = jnp.concatenate([ctab_ref[0] + rt[0:1], ctab_ref[0] + rt[1:2]], axis=0)
    sin = jnp.concatenate([ctab_ref[1] + rt[2:3], ctab_ref[1] + rt[3:4]], axis=0)

    def turn(x, gain):
        x = x.astype(F32)
        sq = x * x
        hi = sq.astype(BF16)
        lo = (sq - hi.astype(F32)).astype(BF16)
        ms = jnp.dot(hi, seg, preferred_element_type=F32) + jnp.dot(
            lo, seg, preferred_element_type=F32
        )
        y = x * lax.rsqrt(ms + EPS) * gain
        swapped = jnp.where(even, pltpu.roll(y, 127, 1), pltpu.roll(y, 1, 1))
        return y * cos + swapped * sin

    kgain = jnp.concatenate([kg_ref[...], kg_ref[...]], axis=1)
    for p in range(2):
        cols = slice(p * 128, (p + 1) * 128)
        kv[p, 0, :, 0:128] = turn(k_ref[0, :, cols], kgain).astype(BF16)
        kv[p, 0, :, 128:256] = v_ref[0, :, cols]
        kv[p, :, :, 256:384] = jnp.ones((16, TOK, 128), BF16)

    pl.semaphore_wait(barrier, len(peers))

    def hop(p, axis, k, src, dst):
        return pltpu.make_async_remote_copy(
            src_ref=kv.at[p, src, :, pl.ds(0, 256)],
            dst_ref=kv.at[p, dst, :, pl.ds(0, 256)],
            send_sem=gs.at[p, dst // 4],
            recv_sem=gr.at[p, min(dst, 12)],
            device_id=dev(axis, k),
            device_id_type=MESH,
        )

    def gather_first(p, k1):
        return hop(p, PAIRS[p][0], k1, 0, k1)

    def gather_second(p, k2, k1):
        if k2 == 2:
            k = 1 if k1 < 2 else 3
            return hop(p, PAIRS[p][1], k, PLACE[k] * 4 + k1, PLACE[2] * 4 + k1)
        return hop(p, PAIRS[p][1], k2, k1, PLACE[k2] * 4 + k1)

    for k1 in NEAR:
        for p in range(2):
            gather_first(p, k1).start()
    for k2 in (1, 3):
        for p in range(2):
            gather_second(p, k2, 0).start()

    loaded(5, 13)
    qgain = jnp.concatenate([qg_ref[...], qg_ref[...]], axis=1)
    for b in range(8):
        t = turn(q_ref[0, :, b * 128 : (b + 1) * 128], qgain).astype(BF16).astype(F32) * 0.125
        flip = pltpu.roll(t, 64, 1)
        p, pos, i = b // 4, (b // 2) % 2, (b % 4) * 2
        if pos == 0:
            a0, a1 = jnp.where(low, t, 0.0), jnp.where(low, flip, 0.0)
        else:
            a0, a1 = jnp.where(low, 0.0, flip), jnp.where(low, 0.0, t)
        qp[p, i * 128 : (i + 1) * 128] = a0.astype(BF16)
        qp[p, (i + 1) * 128 : (i + 2) * 128] = a1.astype(BF16)

    for k1 in (1, 3, 2):
        for p in range(2):
            gather_first(p, k1).wait_recv()
            for k2 in (1, 3):
                gather_second(p, k2, k1).start()
    for p in range(2):
        gather_second(p, 1, 0).wait_recv()
        gather_second(p, 2, 0).start()

    tok_r = lax.broadcasted_iota(jnp.int32, (128, 128), 0)
    tok_c = lax.broadcasted_iota(jnp.int32, (128, 128), 1)
    before = (tok_r < tok_c).astype(F32).astype(BF16)
    idt = [ids_ref[k : k + 1, :] for k in range(2)]
    hot = [(t == tok_r).astype(F32) for t in idt]
    cnt = [jnp.dot(h.astype(BF16), before, preferred_element_type=F32) for h in hot]
    cnt[1] = cnt[1] + jnp.sum(hot[0], axis=1, keepdims=True)
    rank = [jnp.sum(h * c, axis=0, keepdims=True).astype(jnp.int32) for h, c in zip(hot, cnt)]
    slot_row = lax.broadcasted_iota(jnp.int32, (SLOTS, 128), 0)
    slot_col = lax.broadcasted_iota(jnp.int32, (128, SLOTS), 1).astype(F32)
    for p, (axes, _, _) in enumerate(PARTS):
        slots = []
        for k in range(2):
            e = idt[k]
            at = (e // 32, (e // 8) % 4, (e // 2) % 4)
            rel = [(at[a] - mine[a] + 4) % 4 for a in axes]
            kc = (e % 2 + core) % 2
            slots.append((((kc * 4 + rel[0]) * 4 + rel[1]) * 4 + rel[2]) * 4 + rank[k])
        disp[p] = ((slot_row == slots[0]) | (slot_row == slots[1])).astype(F32).astype(BF16)
        for k in range(2):
            col = jnp.transpose(jnp.broadcast_to(slots[k].astype(F32), (128, 128)))[:, 0:1]
            comb[p, k] = (slot_col == col).astype(F32).astype(BF16)

    def stripe(first_place, count, fresh):
        for p in range(2):
            span = slice(first_place * 4, (first_place + count) * 4)
            n = count * 512
            keys = kv[p, span, :, 0:128].reshape(n, 128)
            vals = kv[p, span, :, 128:384].reshape(n, 256)
            for i in range(1024 // ROWS):
                r = slice(i * ROWS, (i + 1) * ROWS)
                sc = lax.dot_general(
                    qp[p, r, :], keys, (((1,), (1,)), ((), ())), preferred_element_type=F32
                )
                top = jnp.broadcast_to(jnp.max(sc, axis=1, keepdims=True), (ROWS, 128))
                if not fresh:
                    old = mx[p, r, :]
                    top = jnp.maximum(top, old)
                    fade = jnp.exp(old - top)
                mx[p, r, :] = top
                e = jnp.exp(sc - jnp.concatenate([top] * (n // 128), axis=1)).astype(BF16)
                o = jnp.dot(e, vals, preferred_element_type=F32)
                if not fresh:
                    o = o + acc[p, r, :] * jnp.concatenate([fade, fade], axis=1)
                acc[p, r, :] = o

    stripe(0, 1, True)
    for k2, k1 in ((1, 1), (3, 3), (3, 2)):
        for p in range(2):
            gather_second(p, k2, k1).wait_recv()
            gather_second(p, 2, k1).start()
    for k2, rest in ((1, (3, 2)), (3, (0, 1))):
        for k1 in rest:
            for p in range(2):
                gather_second(p, k2, k1).wait_recv()
    stripe(1, 2, False)
    for p in range(2):
        drain(kv.at[p, pl.ds(12, 4), :, pl.ds(0, 256)], gr.at[p, 12])
    stripe(3, 1, False)

    for b in range(8):
        p, pos, i = b // 4, (b // 2) % 2, (b % 4) * 2
        o = []
        for j in (i, i + 1):
            r = slice(j * 128, (j + 1) * 128)
            o.append(acc[p, r, 0:128] / acc[p, r, 128:256])
        if pos == 0:
            a = jnp.where(low, o[0], pltpu.roll(o[1], 64, 1))
        else:
            a = jnp.where(low, pltpu.roll(o[0], 64, 1), o[1])
        att[:, b * 128 : (b + 1) * 128] = a.astype(BF16)

    loaded(13, 14)
    projected = jnp.dot(att[...], wo[...], preferred_element_type=F32)
    fr = (res_ref[0].astype(F32) + rms(projected) * mix_ref[...]).astype(BF16)
    first[...] = fr
    normed[...] = (rms(fr.astype(F32)) * ffn_ref[...]).astype(BF16)

    def cols_of(p):
        return pl.ds(PARTS[p][1], PARTS[p][2])

    def remote(src, dst, ss, rs, device):
        return pltpu.make_async_remote_copy(
            src_ref=src, dst_ref=dst, send_sem=ss, recv_sem=rs, device_id=device, device_id_type=MESH
        )

    def stage1(u, k1, back):
        w, p = u
        n = w * 3 + p
        axis = PARTS[p][0][0]
        c = cols_of(p)
        if back:
            src, dst = inboxr.at[w, k1, :, c], outr.at[w, k1, :, c]
            if k1 == 0:
                return pltpu.make_async_copy(src, dst, r3r.at[n])
            return remote(src, dst, sent.at[n, 1], r3r.at[n], dev(axis, 4 - k1))
        return remote(outbox.at[w, k1, :, c], inbox.at[w, k1, :, c], sent.at[n, 0], f1r.at[n, k1 - 1], dev(axis, k1))

    def stage2(u, k2, k1, back):
        w, p = u
        n = w * 3 + p
        axis = PARTS[p][0][1]
        c = cols_of(p)
        r = pl.ds(k2 * 16, 16)
        if back:
            return remote(midr.at[w, k2, k1, :, c], inboxr.at[w, k1, r, c], sent.at[n, 1], r2r.at[n, k1], dev(axis, 4 - k2))
        g = k1 if p == 2 else k2
        return remote(inbox.at[w, k1, r, c], mid.at[w, k2, k1, :, c], sent.at[n, 0], f2r.at[n, g], dev(axis, k2))

    def stage3(u, g, zero, k3, back):
        w, p = u
        n = w * 3 + p
        axis = PARTS[p][0][2]
        c = cols_of(p)
        r = pl.ds(k3 * 4, 4)
        box, deep, far = (inboxr, midr, ys) if back else (inbox, mid, xs)
        if p == 2:
            q = pl.ds(g * 4, 4)
            if zero:
                here, there = box.at[w, g, r, c], far.at[w, k3, 0, q, c]
            else:
                here, there = deep.at[w, pl.ds(1, 3), g, r, c], far.at[w, k3, pl.ds(1, 3), q, c]
        else:
            here = box.at[w, :, r, c] if zero else deep.at[w, g, :, r, c]
            there = far.at[w, g, :, r, c] if p == 0 else far.at[w, :, k3, pl.ds(g * 4, 4), c]
        if back:
            sem = r1z.at[n] if zero else r1r.at[n, g]
            if (k3, w) == (0, 0):
                return pltpu.make_async_copy(there, here, sem)
            return remote(there, here, sent.at[n, 1], sem, dev(axis, 4 - k3, w))
        if (k3, w) == (0, 0):
            return pltpu.make_async_copy(here, there, f3r.at[n])
        return remote(here, there, sent.at[n, 0], f3r.at[n], dev(axis, k3, w))

    def fan(u, g, zero, back):
        for k3 in NEAR + (0,):
            stage3(u, g, zero, k3, back).start()

    for u in UNITS:
        w, p = u
        c = slice(PARTS[p][1], PARTS[p][1] + PARTS[p][2])
        packed = (
            jnp.dot(disp[p, w * 256 : (w + 1) * 256], normed[:, c], preferred_element_type=F32)
            .astype(BF16)
            .reshape(4, 64, PARTS[p][2])
        )
        inbox[w, 0, :, c] = packed[0]
        outbox[w, 1:4, :, c] = packed[1:4]
        for k1 in NEAR:
            stage1(u, k1, False).start()
        for k2 in NEAR:
            stage2(u, k2, 0, False).start()
    for w in range(2):
        for k1 in (1, 3, 2):
            for p in range(3):
                u = (w, p)
                drain(inbox.at[w, k1, :, cols_of(p)], f1r.at[w * 3 + p, k1 - 1])
                for k2 in NEAR:
                    stage2(u, k2, k1, False).start()
        for p in range(3):
            u = (w, p)
            for g in range(4) if p == 2 else range(1):
                fan(u, g, True, False)
    for w in range(2):
        for i in range(4):
            for p in range(3):
                u = (w, p)
                n = w * 3 + p
                c = cols_of(p)
                if p == 2:
                    g = (0, 1, 3, 2)[i]
                    drain(mid.at[w, pl.ds(1, 3), g, :, c], f2r.at[n, g])
                    fan(u, g, False, False)
                elif i > 0:
                    g = (0, 1, 3, 2)[i]
                    drain(mid.at[w, g, :, :, c], f2r.at[n, g])
                    fan(u, g, False, False)

    for w in range(2):
        if w == 0:
            loaded(14, 17)
        for p in range(3):
            drain(xs.at[w, :, :, :, cols_of(p)], f3r.at[w * 3 + p])
        x = xs[w].reshape(256, D)
        gate = jnp.dot(x, wg[...], preferred_element_type=F32)
        up = jnp.dot(x, wu[...], preferred_element_type=F32)
        hidden = (jax.nn.silu(gate) * up).astype(BF16)
        for p in range(3):
            u = (w, p)
            c = slice(PARTS[p][1], PARTS[p][1] + PARTS[p][2])
            ys[w, :, :, :, c] = (
                jnp.dot(hidden, wd[:, c], preferred_element_type=F32)
                .astype(BF16)
                .reshape(4, 4, 16, PARTS[p][2])
            )
            for g in NEAR + (0,):
                if p == 2 or g > 0:
                    fan(u, g, False, True)
            for g in range(4) if p == 2 else range(1):
                fan(u, g, True, True)

    for w in range(2):
        for i in range(4):
            for p in range(3):
                u = (w, p)
                n = w * 3 + p
                c = cols_of(p)
                g = (NEAR + (0,))[i]
                if p == 2:
                    drain(midr.at[w, pl.ds(1, 3), g, :, c], r1r.at[n, g])
                    for k2 in NEAR:
                        stage2(u, k2, g, True).start()
                elif g > 0:
                    drain(midr.at[w, g, :, :, c], r1r.at[n, g])
                    for k1 in NEAR + (0,):
                        stage2(u, g, k1, True).start()
    for w in range(2):
        for p in range(3):
            drain(inboxr.at[w, :, pl.ds(0, 16), cols_of(p)], r1z.at[w * 3 + p])
        for k1 in NEAR + (0,):
            for p in range(3):
                drain(inboxr.at[w, k1, pl.ds(16, 48), cols_of(p)], r2r.at[w * 3 + p, k1])
                stage1((w, p), k1, True).start()

    g0, g1 = [jnp.transpose(jnp.broadcast_to(gate_ref[k : k + 1, :], (128, 128))) for k in range(2)]
    sums = [None] * 3
    for w in range(2):
        for p in range(3):
            c = slice(PARTS[p][1], PARTS[p][1] + PARTS[p][2])
            half = slice(w * 256, (w + 1) * 256)
            wide = PARTS[p][2] // 128
            drain(outr.at[w, :, :, cols_of(p)], r3r.at[w * 3 + p])
            back = outr[w, :, :, c].reshape(256, PARTS[p][2])
            a0 = jnp.dot(comb[p, 0, :, half], back, preferred_element_type=F32)
            a1 = jnp.dot(comb[p, 1, :, half], back, preferred_element_type=F32)
            term = jnp.concatenate([g0] * wide, axis=1) * a0 + jnp.concatenate([g1] * wide, axis=1) * a1
            if w == 0:
                tot[:, c] = term
            else:
                sums[p] = tot[:, c] + term
    total = jnp.concatenate(sums, axis=1)
    out_ref[0] = (first[...].astype(F32) + rms(total) * post_ref[...]).astype(BF16)

    for p in range(2):
        drain(kv.at[p, pl.ds(0, 3), :, pl.ds(0, 256)], gs.at[p, 0])
        for i in range(1, 4):
            drain(kv.at[p, pl.ds(0, 4), :, pl.ds(0, 256)], gs.at[p, i])
    for w, p in UNITS:
        n = w * 3 + p
        c = cols_of(p)
        for i in range(2):
            drain(wo.at[pl.ds(0, 576 + w * 64), c], sent.at[n, i])


def shards(
    queries, keys, values, q_gain, k_gain, residual, out_weight, mix_gain, ffn_gain, post_gain,
    expert_ids, expert_gate, w_gate, w_up, w_down,
):
    rows, cols = tables()
    vm = pl.BlockSpec(memory_space=pltpu.VMEM)
    hbm = pl.BlockSpec(memory_space=pltpu.HBM)
    sem = pltpu.SemaphoreType.DMA
    box = pltpu.VMEM((2, 4, 64, D), BF16)
    deep = pltpu.VMEM((2, 4, 4, 16, D), BF16)
    return pl.pallas_call(
        kernel,
        out_shape=jax.ShapeDtypeStruct((1, TOK, D), BF16),
        in_specs=[hbm] * 17,
        out_specs=vm,
        scratch_shapes=[
            pltpu.VMEM((1, TOK, 256), BF16), pltpu.VMEM((1, TOK, 256), BF16), pltpu.VMEM((1, 64), F32),
            pltpu.VMEM((16, 8, 128), F32), pltpu.VMEM((2, 64, 128), F32),
            pltpu.VMEM((1, TOK, 1024), BF16), pltpu.VMEM((1, 64), F32),
            pltpu.VMEM((2, TOK), jnp.int32), pltpu.VMEM((2, TOK), F32), pltpu.VMEM((1, TOK, D), BF16),
            pltpu.VMEM((1, D), F32), pltpu.VMEM((1, D), F32), pltpu.VMEM((1, D), F32),
            pltpu.VMEM((1024, D), BF16),
            pltpu.VMEM((D, 512), BF16),
            pltpu.VMEM((D, 512), BF16),
            pltpu.VMEM((512, D), BF16),
            pltpu.VMEM((2, 1024, 128), BF16),
            pltpu.VMEM((2, 16, TOK, 384), BF16),
            pltpu.VMEM((2, 1024, 128), F32),
            pltpu.VMEM((2, 1024, 256), F32),
            pltpu.VMEM((TOK, 1024), BF16),
            pltpu.VMEM((TOK, D), BF16),
            pltpu.VMEM((TOK, D), BF16),
            pltpu.VMEM((3, SLOTS, 128), BF16),
            pltpu.VMEM((3, 2, 128, SLOTS), BF16),
            box, box, deep, deep, deep, deep, box, box,
            pltpu.VMEM((TOK, D), F32),
            sem((17,)),
            sem((2, 4)), sem((2, 13)),
            sem((6, 3)), sem((6, 4)), sem((6,)),
            sem((6, 4)), sem((6,)), sem((6, 4)), sem((6,)),
            sem((6, 2)),
        ],
        compiler_params=pltpu.CompilerParams(
            collective_id=0, has_side_effects=True, vmem_limit_bytes=LIMIT
        ),
        name="layer",
    )(
        keys, values, k_gain[None], jnp.asarray(rows), jnp.asarray(cols), queries, q_gain[None],
        expert_ids[0].T, expert_gate[0].T, residual, mix_gain[None], ffn_gain[None], post_gain[None],
        out_weight, w_gate, w_up, w_down,
    )


def solution(mesh):
    return jax.shard_map(
        shards,
        mesh=mesh,
        in_specs=(
            P("dp", "sp", None), P("dp", "sp", None), P("dp", "sp", None), P(), P(),
            P("dp", "sp", None), P(), P(), P(), P(),
            P("dp", "sp", None), P("dp", "sp", None),
            P(("sp", "dp"), None, None), P(("sp", "dp"), None, None), P(("sp", "dp"), None, None),
        ),
        out_specs=P("dp", "sp", None),
        check_vma=False,
    )
```

time: 89.5 us -> 81.4 us (0.909)
  Pallas kernels: 86.7 us -> 78.4 us
    pallas_call x1, Pallas kernels: 86.7 us -> 78.4 us  [shards(): pl.pallas_call(kernel, out_shape=jax.ShapeDtypeStruct((1, TOK, D), BF16),...]
where the time goes in v3:
time: 81.4 us; the launch traced here: 80.3 us
  Pallas kernels  78.4 us (96%)
  local copies, waits for them, and re-layouts  1.88 us (2%)
    pallas_call x1, Pallas kernels, shards(): pl.pallas_call(kernel, out_shape=jax.ShapeDtypeStruct((1, TOK, D), BF16),...  78.4 us
    unnamed x1, local copies, waits for them, and re-layouts  1.88 us

profile of v3, /device:TPU:0, one launch (start us, length us, event | category | flops | bytes accessed | tf_op | source)
XLA Modules:
  0.0 80.3 jit_solution(3909995471392416618)
XLA Ops:
  0.0 78.4 %layer.1 = bf16[1,128,2048]{2,1,0:T(8,128)(2,1)} custom-call(bf16[1,128,256]{2,1,0:T(8,128)(2,1)} %k_hbm.1, bf16[1,128,256]{2,1,0:T(8,128)(2,1)} %v_hbm.1, f32[1,64]{1,0:T(1,128)} %bitcast.16, f32[16,8,128]{2,1,0:T(8,128)} %constant.4.clone.rtab_hbm, f32[2,64,128]{2,1,0:T(8,128)} %constant.5.clone.ctab_hbm, bf16[1,128,1024]{2,1,0:T(8,128)(2,1)} %q_hbm.1, ...), custom_call_target="tpu_custom_call" | custom-call | tf_op jit(solution)/shard_map/layer/pallas_call | solution.py:444
  78.4 1.9 %copy.19 = bf16[1,128,2048]{2,1,0:T(8,128)(2,1)} copy(bf16[1,128,2048]{2,1,0:T(8,128)(2,1)} %layer.1) | data formatting | bytes 1048576

commit v4 on v3

--- a/solution.py
+++ b/solution.py
@@ -20,7 +20,10 @@
 
 PARTS = (((0, 1, 2), 0, 640), ((1, 2, 0), 640, 640), ((2, 0, 1), 1280, 768))
 UNITS = tuple((w, p) for w in range(2) for p in range(3))
-PLACE = {0: 0, 1: 1, 3: 2, 2: 3}
+PLACE = {
+    (0, 0): 0, (0, 1): 1, (0, 2): 2, (0, 3): 3, (1, 0): 4, (3, 0): 5, (1, 1): 6, (3, 1): 7,
+    (1, 3): 8, (3, 3): 9, (1, 2): 10, (3, 2): 11, (2, 0): 12, (2, 1): 13, (2, 2): 14, (2, 3): 15,
+}
 PAIRS = ((0, 1), (1, 0))
 NEAR = (2, 1, 3)
 
@@ -55,8 +58,8 @@
     k_ref, v_ref, kg_ref, rtab_ref, ctab_ref, q_ref, qg_ref, ids_ref, gate_ref, res_ref,
     mix_ref, ffn_ref, post_ref,
     wo, wg, wu, wd, qp, kv, mx, acc, att, first, normed, disp, comb,
-    outbox, inbox, mid, xs, ys, midr, inboxr, outr, tot,
-    wsem, gs, gr, f1r, f2r, f3r, r1r, r1z, r2r, r3r, sent,
+    ids_in, line, inbox, mid, xs, ys, midr, inboxr, outr, tot,
+    wsem, idsem, gs, gr, f1s, f1r, f2r, f3r, r1r, r1z, r2r, r3r, sent,
 ):
     s = lax.axis_index("sp")
     d = lax.axis_index("dp")
@@ -81,7 +84,7 @@
         for i, (src, dst) in enumerate(
             (
                 (k_hbm, k_ref), (v_hbm, v_ref), (kg_hbm, kg_ref), (rtab_hbm, rtab_ref), (ctab_hbm, ctab_ref),
-                (q_hbm, q_ref), (qg_hbm, qg_ref), (ids_hbm, ids_ref), (gate_hbm, gate_ref), (res_hbm, res_ref),
+                (ids_hbm, ids_ref), (q_hbm, q_ref), (qg_hbm, qg_ref), (gate_hbm, gate_ref), (res_hbm, res_ref),
                 (mix_hbm, mix_ref), (ffn_hbm, ffn_ref), (post_hbm, post_ref),
                 (wo_hbm, wo), (wg_hbm.at[0], wg), (wu_hbm.at[0], wu), (wd_hbm.at[0], wd),
             )
@@ -103,7 +106,7 @@
         1.0 / 64.0,
         0.0,
     ).astype(BF16)
-    loaded(0, 5)
+    loaded(0, 6)
     rt = rtab_ref[s]
     cos = jnp.concatenate([ctab_ref[0] + rt[0:1], ctab_ref[0] + rt[1:2]], axis=0)
     sin = jnp.concatenate([ctab_ref[1] + rt[2:3], ctab_ref[1] + rt[3:4]], axis=0)
@@ -145,8 +148,8 @@
     def gather_second(p, k2, k1):
         if k2 == 2:
             k = 1 if k1 < 2 else 3
-            return hop(p, PAIRS[p][1], k, PLACE[k] * 4 + k1, PLACE[2] * 4 + k1)
-        return hop(p, PAIRS[p][1], k2, k1, PLACE[k2] * 4 + k1)
+            return hop(p, PAIRS[p][1], k, PLACE[k, k1], PLACE[2, k1])
+        return hop(p, PAIRS[p][1], k2, k1, PLACE[k2, k1])
 
     for k1 in NEAR:
         for p in range(2):
@@ -155,7 +158,18 @@
         for p in range(2):
             gather_second(p, k2, 0).start()
 
-    loaded(5, 13)
+    for axis in range(3):
+        for k in NEAR:
+            pltpu.make_async_remote_copy(
+                src_ref=ids_ref,
+                dst_ref=ids_in.at[axis, k],
+                send_sem=idsem.at[0],
+                recv_sem=idsem.at[1],
+                device_id=dev(axis, k),
+                device_id_type=MESH,
+            ).start()
+
+    loaded(6, 13)
     qgain = jnp.concatenate([qg_ref[...], qg_ref[...]], axis=1)
     for b in range(8):
         t = turn(q_ref[0, :, b * 128 : (b + 1) * 128], qgain).astype(BF16).astype(F32) * 0.125
@@ -180,24 +194,36 @@
     tok_r = lax.broadcasted_iota(jnp.int32, (128, 128), 0)
     tok_c = lax.broadcasted_iota(jnp.int32, (128, 128), 1)
     before = (tok_r < tok_c).astype(F32).astype(BF16)
-    idt = [ids_ref[k : k + 1, :] for k in range(2)]
-    hot = [(t == tok_r).astype(F32) for t in idt]
-    cnt = [jnp.dot(h.astype(BF16), before, preferred_element_type=F32) for h in hot]
-    cnt[1] = cnt[1] + jnp.sum(hot[0], axis=1, keepdims=True)
-    rank = [jnp.sum(h * c, axis=0, keepdims=True).astype(jnp.int32) for h, c in zip(hot, cnt)]
-    slot_row = lax.broadcasted_iota(jnp.int32, (SLOTS, 128), 0)
+    slot_row = lax.broadcasted_iota(jnp.int32, (128, 128), 0)
     slot_col = lax.broadcasted_iota(jnp.int32, (128, SLOTS), 1).astype(F32)
+
+    def route(pair):
+        idt = [pair[k : k + 1, :] for k in range(2)]
+        hot = [(t == tok_r).astype(F32) for t in idt]
+        cnt = [jnp.dot(h.astype(BF16), before, preferred_element_type=F32) for h in hot]
+        cnt[1] = cnt[1] + jnp.sum(hot[0], axis=1, keepdims=True)
+        rank = [jnp.sum(h * c, axis=0, keepdims=True).astype(jnp.int32) for h, c in zip(hot, cnt)]
+        return list(zip(idt, rank))
+
+    def places(e, rank, axes):
+        at = (e // 32, (e // 8) % 4, (e // 2) % 4)
+        rel = [(at[a] - mine[a] + 4) % 4 for a in axes]
+        return rel[0], (e % 2 + core) % 2, (rel[1] * 4 + rel[2]) * 4 + rank
+
+    def pick(p, k, routed):
+        slots = []
+        for e, rank in routed:
+            plane, kc, r = places(e, rank, PARTS[p][0])
+            slots.append(jnp.where(plane == 0, kc * 64 + r, -1))
+        disp[p, k] = ((slot_row == slots[0]) | (slot_row == slots[1])).astype(F32).astype(BF16)
+
+    own = route(ids_ref[...])
     for p, (axes, _, _) in enumerate(PARTS):
-        slots = []
-        for k in range(2):
-            e = idt[k]
-            at = (e // 32, (e // 8) % 4, (e // 2) % 4)
-            rel = [(at[a] - mine[a] + 4) % 4 for a in axes]
-            kc = (e % 2 + core) % 2
-            slots.append((((kc * 4 + rel[0]) * 4 + rel[1]) * 4 + rel[2]) * 4 + rank[k])
-        disp[p] = ((slot_row == slots[0]) | (slot_row == slots[1])).astype(F32).astype(BF16)
-        for k in range(2):
-            col = jnp.transpose(jnp.broadcast_to(slots[k].astype(F32), (128, 128)))[:, 0:1]
+        pick(p, 0, own)
+        for k, (e, rank) in enumerate(own):
+            plane, kc, r = places(e, rank, axes)
+            full = (kc * 4 + plane) * 64 + r
+            col = jnp.transpose(jnp.broadcast_to(full.astype(F32), (128, 128)))[:, 0:1]
             comb[p, k] = (slot_col == col).astype(F32).astype(BF16)
 
     def stripe(first_place, count, fresh):
@@ -224,15 +250,28 @@
                 acc[p, r, :] = o
 
     stripe(0, 1, True)
-    for k2, k1 in ((1, 1), (3, 3), (3, 2)):
+
+    def relay(k2, k1):
         for p in range(2):
             gather_second(p, k2, k1).wait_recv()
             gather_second(p, 2, k1).start()
-    for k2, rest in ((1, (3, 2)), (3, (0, 1))):
-        for k1 in rest:
+
+    def arrive(*pieces):
+        for k2, k1 in pieces:
             for p in range(2):
                 gather_second(p, k2, k1).wait_recv()
-    stripe(1, 2, False)
+
+    relay(1, 1)
+    drain(ids_in.at[:, pl.ds(1, 3)], idsem.at[1])
+    for p in range(3):
+        for k in NEAR:
+            pick(p, k, route(ids_in[p, k]))
+    relay(3, 3)
+    arrive((3, 0), (3, 1))
+    stripe(1, 1, False)
+    relay(3, 2)
+    arrive((1, 3), (1, 2))
+    stripe(2, 1, False)
     for p in range(2):
         drain(kv.at[p, pl.ds(12, 4), :, pl.ds(0, 256)], gr.at[p, 12])
     stripe(3, 1, False)
@@ -263,17 +302,22 @@
             src_ref=src, dst_ref=dst, send_sem=ss, recv_sem=rs, device_id=device, device_id_type=MESH
         )
 
-    def stage1(u, k1, back):
+    def stage1(p, k1, relayed):
+        axis = PARTS[p][0][0]
+        c = cols_of(p)
+        if relayed:
+            r = pl.ds(0 if k1 == 1 else 64, 64)
+            return remote(line.at[k1, r, c], line.at[2, r, c], f1s.at[p], f1r.at[p, 1], dev(axis, k1))
+        return remote(normed.at[:, c], line.at[k1, :, c], f1s.at[p], f1r.at[p, k1 - 1], dev(axis, k1))
+
+    def last1(u, k1):
         w, p = u
         n = w * 3 + p
-        axis = PARTS[p][0][0]
         c = cols_of(p)
-        if back:
-            src, dst = inboxr.at[w, k1, :, c], outr.at[w, k1, :, c]
-            if k1 == 0:
-                return pltpu.make_async_copy(src, dst, r3r.at[n])
-            return remote(src, dst, sent.at[n, 1], r3r.at[n], dev(axis, 4 - k1))
-        return remote(outbox.at[w, k1, :, c], inbox.at[w, k1, :, c], sent.at[n, 0], f1r.at[n, k1 - 1], dev(axis, k1))
+        src, dst = inboxr.at[w, k1, :, c], outr.at[w, k1, :, c]
+        if k1 == 0:
+            return pltpu.make_async_copy(src, dst, r3r.at[n])
+        return remote(src, dst, sent.at[n, 1], r3r.at[n], dev(PARTS[p][0][0], 4 - k1))
 
     def stage2(u, k2, k1, back):
         w, p = u
@@ -304,7 +348,7 @@
             there = far.at[w, g, :, r, c] if p == 0 else far.at[w, :, k3, pl.ds(g * 4, 4), c]
         if back:
             sem = r1z.at[n] if zero else r1r.at[n, g]
-            if (k3, w) == (0, 0):
+            if k3 == 0 and w == 0:
                 return pltpu.make_async_copy(there, here, sem)
             return remote(there, here, sent.at[n, 1], sem, dev(axis, 4 - k3, w))
         if (k3, w) == (0, 0):
@@ -312,51 +356,94 @@
         return remote(here, there, sent.at[n, 0], f3r.at[n], dev(axis, k3, w))
 
     def fan(u, g, zero, back):
-        for k3 in NEAR + (0,):
-            stage3(u, g, zero, k3, back).start()
-
-    for u in UNITS:
-        w, p = u
+        if not back:
+            return [(k3, stage3(u, g, zero, k3, back)) for k3 in (1, 3, 0, 2)]
+
+        @pl.when(u[0] == 0)
+        def _():
+            stage3((0, u[1]), g, zero, 0, back).start()
+
+        @pl.when(u[0] == 1)
+        def _():
+            stage3((1, u[1]), g, zero, 0, back).start()
+
+        return [(k3, stage3(u, g, zero, k3, back)) for k3 in (1, 3, 2)]
+
+    def go(items):
+        for far in (False, True):
+            for k, copy in items:
+                if (k == 2) == far:
+                    copy.start()
+
+    for k1 in (1, 3):
+        for p in range(3):
+            stage1(p, k1, False).start()
+
+    def pack(p, k1):
         c = slice(PARTS[p][1], PARTS[p][1] + PARTS[p][2])
-        packed = (
-            jnp.dot(disp[p, w * 256 : (w + 1) * 256], normed[:, c], preferred_element_type=F32)
-            .astype(BF16)
-            .reshape(4, 64, PARTS[p][2])
-        )
-        inbox[w, 0, :, c] = packed[0]
-        outbox[w, 1:4, :, c] = packed[1:4]
-        for k1 in NEAR:
-            stage1(u, k1, False).start()
-        for k2 in NEAR:
-            stage2(u, k2, 0, False).start()
+        rows = normed[:, c] if k1 == 0 else line[k1, :, c]
+        packed = jnp.dot(disp[p, k1], rows, preferred_element_type=F32).astype(BF16)
+        inbox[:, k1, :, c] = packed.reshape(2, 64, PARTS[p][2])
+        return [(k2, stage2((w, p), k2, k1, False)) for w in range(2) for k2 in (1, 3, 2)]
+
+    def packs(k1):
+        items = []
+        for p in range(3):
+            items += pack(p, k1)
+        go(items)
+
+    packs(0)
+    for k1 in (1, 3):
+        for p in range(3):
+            drain(line.at[k1, :, cols_of(p)], f1r.at[p, k1 - 1])
+            stage1(p, k1, True).start()
+    packs(1)
+    packs(3)
+    for p in range(3):
+        drain(line.at[2, :, cols_of(p)], f1r.at[p, 1])
+    packs(2)
     for w in range(2):
-        for k1 in (1, 3, 2):
-            for p in range(3):
-                u = (w, p)
-                drain(inbox.at[w, k1, :, cols_of(p)], f1r.at[w * 3 + p, k1 - 1])
-                for k2 in NEAR:
-                    stage2(u, k2, k1, False).start()
-        for p in range(3):
-            u = (w, p)
+        items = []
+        for p in range(3):
             for g in range(4) if p == 2 else range(1):
-                fan(u, g, True, False)
+                items += fan((w, p), g, True, False)
+        go(items)
     for w in range(2):
         for i in range(4):
+            items = []
             for p in range(3):
                 u = (w, p)
                 n = w * 3 + p
                 c = cols_of(p)
+                g = (0, 1, 3, 2)[i]
                 if p == 2:
-                    g = (0, 1, 3, 2)[i]
                     drain(mid.at[w, pl.ds(1, 3), g, :, c], f2r.at[n, g])
-                    fan(u, g, False, False)
                 elif i > 0:
-                    g = (0, 1, 3, 2)[i]
                     drain(mid.at[w, g, :, :, c], f2r.at[n, g])
-                    fan(u, g, False, False)
-
-    for w in range(2):
-        if w == 0:
+                if p == 2 or i > 0:
+                    items += fan(u, g, False, False)
+            go(items)
+
+    def middle():
+        for w in range(2):
+            for i in range(4):
+                items = []
+                for p in range(3):
+                    u = (w, p)
+                    n = w * 3 + p
+                    c = cols_of(p)
+                    g = (NEAR + (0,))[i]
+                    if p == 2:
+                        drain(midr.at[w, pl.ds(1, 3), g, :, c], r1r.at[n, g])
+                        items += [(k2, stage2(u, k2, g, True)) for k2 in (1, 3, 2)]
+                    elif g > 0:
+                        drain(midr.at[w, g, :, :, c], r1r.at[n, g])
+                        items += [(g, stage2(u, g, k1, True)) for k1 in NEAR + (0,)]
+                go(items)
+
+    for turn_no in range(2):
+        w = (1 - core + turn_no) % 2
+        if turn_no == 0:
             loaded(14, 17)
         for p in range(3):
             drain(xs.at[w, :, :, :, cols_of(p)], f3r.at[w * 3 + p])
@@ -372,34 +459,25 @@
                 .astype(BF16)
                 .reshape(4, 4, 16, PARTS[p][2])
             )
+            items = []
             for g in NEAR + (0,):
                 if p == 2 or g > 0:
-                    fan(u, g, False, True)
+                    items += fan(u, g, False, True)
             for g in range(4) if p == 2 else range(1):
-                fan(u, g, True, True)
-
-    for w in range(2):
-        for i in range(4):
-            for p in range(3):
-                u = (w, p)
-                n = w * 3 + p
-                c = cols_of(p)
-                g = (NEAR + (0,))[i]
-                if p == 2:
-                    drain(midr.at[w, pl.ds(1, 3), g, :, c], r1r.at[n, g])
-                    for k2 in NEAR:
-                        stage2(u, k2, g, True).start()
-                elif g > 0:
-                    drain(midr.at[w, g, :, :, c], r1r.at[n, g])
-                    for k1 in NEAR + (0,):
-                        stage2(u, g, k1, True).start()
+                items += fan(u, g, True, True)
+            go(items)
+        if turn_no == 0:
+            pl.when(core == 1)(middle)
+        else:
+            pl.when(core == 0)(middle)
+
     for w in range(2):
         for p in range(3):
             drain(inboxr.at[w, :, pl.ds(0, 16), cols_of(p)], r1z.at[w * 3 + p])
         for k1 in NEAR + (0,):
             for p in range(3):
                 drain(inboxr.at[w, k1, pl.ds(16, 48), cols_of(p)], r2r.at[w * 3 + p, k1])
-                stage1((w, p), k1, True).start()
+                last1((w, p), k1).start()
 
     g0, g1 = [jnp.transpose(jnp.broadcast_to(gate_ref[k : k + 1, :], (128, 128))) for k in range(2)]
     sums = [None] * 3
@@ -424,11 +502,14 @@
         drain(kv.at[p, pl.ds(0, 3), :, pl.ds(0, 256)], gs.at[p, 0])
         for i in range(1, 4):
             drain(kv.at[p, pl.ds(0, 4), :, pl.ds(0, 256)], gs.at[p, i])
+    drain(ids_in.at[:, pl.ds(1, 3)], idsem.at[0])
+    for p in range(3):
+        drain(wo.at[pl.ds(0, 384), cols_of(p)], f1s.at[p])
     for w, p in UNITS:
         n = w * 3 + p
         c = cols_of(p)
-        for i in range(2):
-            drain(wo.at[pl.ds(0, 576 + w * 64), c], sent.at[n, i])
+        drain(wo.at[pl.ds(0, 384 + w * 64), c], sent.at[n, 0])
+        drain(wo.at[pl.ds(0, 576 + w * 64), c], sent.at[n, 1])
 
 
 def shards(
@@ -463,13 +544,15 @@
             pltpu.VMEM((TOK, 1024), BF16),
             pltpu.VMEM((TOK, D), BF16),
             pltpu.VMEM((TOK, D), BF16),
-            pltpu.VMEM((3, SLOTS, 128), BF16),
+            pltpu.VMEM((3, 4, 128, 128), BF16),
             pltpu.VMEM((3, 2, 128, SLOTS), BF16),
-            box, box, deep, deep, deep, deep, box, box,
+            pltpu.VMEM((3, 4, 2, TOK), jnp.int32),
+            pltpu.VMEM((4, TOK, D), BF16),
+            box, deep, deep, deep, deep, box, box,
             pltpu.VMEM((TOK, D), F32),
-            sem((17,)),
+            sem((17,)), sem((2,)),
             sem((2, 4)), sem((2, 13)),
-            sem((6, 3)), sem((6, 4)), sem((6,)),
+            sem((3,)), sem((3, 3)), sem((6, 4)), sem((6,)),
             sem((6, 4)), sem((6,)), sem((6, 4)), sem((6,)),
             sem((6, 2)),
         ],

time: 81.4 us -> 79.1 us (0.972); the launches traced: 80.3 us -> 79 us
  Pallas kernels: 78.4 us -> 77.1 us
    pallas_call x1, Pallas kernels: 78.4 us -> 77.1 us  [shards(): pl.pallas_call(kernel, out_shape=jax.ShapeDtypeStruct((1, TOK, D), BF16),...]
where the time goes in v4:
time: 79.1 us; the launch traced here: 79 us
  Pallas kernels  77.1 us (97%)
  local copies, waits for them, and re-layouts  1.88 us (2%)
    pallas_call x1, Pallas kernels, shards(): pl.pallas_call(kernel, out_shape=jax.ShapeDtypeStruct((1, TOK, D), BF16),...  77.1 us
    unnamed x1, local copies, waits for them, and re-layouts  1.88 us

profile of v4, /device:TPU:0, one launch (start us, length us, event | category | flops | bytes accessed | tf_op | source)
XLA Modules:
  0.0 79.0 jit_solution(6723958796035232546)
XLA Ops:
  0.0 77.1 %layer.1 = bf16[1,128,2048]{2,1,0:T(8,128)(2,1)} custom-call(bf16[1,128,256]{2,1,0:T(8,128)(2,1)} %k_hbm.1, bf16[1,128,256]{2,1,0:T(8,128)(2,1)} %v_hbm.1, f32[1,64]{1,0:T(1,128)} %bitcast.16, f32[16,8,128]{2,1,0:T(8,128)} %constant.4.clone.rtab_hbm, f32[2,64,128]{2,1,0:T(8,128)} %constant.5.clone.ctab_hbm, bf16[1,128,1024]{2,1,0:T(8,128)(2,1)} %q_hbm.1, ...), custom_call_target="tpu_custom_call" | custom-call | tf_op jit(solution)/shard_map/layer/pallas_call | solution.py:525
  77.1 1.9 %copy.19 = bf16[1,128,2048]{2,1,0:T(8,128)(2,1)} copy(bf16[1,128,2048]{2,1,0:T(8,128)(2,1)} %layer.1) | data formatting | bytes 1048576

commit v5 on v4

--- a/solution.py
+++ b/solution.py
@@ -424,8 +424,8 @@
                     items += fan(u, g, False, False)
             go(items)
 
-    def middle():
-        for w in range(2):
+    def middle(waves):
+        for w in waves:
             for i in range(4):
                 items = []
                 for p in range(3):
@@ -467,9 +467,10 @@
                 items += fan(u, g, True, True)
             go(items)
         if turn_no == 0:
-            pl.when(core == 1)(middle)
+            pl.when(core == 1)(lambda: middle((0,)))
         else:
-            pl.when(core == 0)(middle)
+            pl.when(core == 1)(lambda: middle((1,)))
+            pl.when(core == 0)(lambda: middle((0, 1)))
 
     for w in range(2):
         for p in range(3):

time: 79.1 us -> 78.1 us (0.987)
  Pallas kernels: 77.1 us -> 76 us
    pallas_call x1, Pallas kernels: 77.1 us -> 76 us  [shards(): pl.pallas_call(kernel, out_shape=jax.ShapeDtypeStruct((1, TOK, D), BF16),...]
where the time goes in v5:
time: 78.1 us; the launch traced here: 77.9 us
  Pallas kernels  76 us (97%)
  local copies, waits for them, and re-layouts  1.88 us (2%)
    pallas_call x1, Pallas kernels, shards(): pl.pallas_call(kernel, out_shape=jax.ShapeDtypeStruct((1, TOK, D), BF16),...  76 us
    unnamed x1, local copies, waits for them, and re-layouts  1.88 us

profile of v5, /device:TPU:0, one launch (start us, length us, event | category | flops | bytes accessed | tf_op | source)
XLA Modules:
  0.0 77.9 jit_solution(4928650599627746018)
XLA Ops:
  0.0 76.0 %layer.1 = bf16[1,128,2048]{2,1,0:T(8,128)(2,1)} custom-call(bf16[1,128,256]{2,1,0:T(8,128)(2,1)} %k_hbm.1, bf16[1,128,256]{2,1,0:T(8,128)(2,1)} %v_hbm.1, f32[1,64]{1,0:T(1,128)} %bitcast.16, f32[16,8,128]{2,1,0:T(8,128)} %constant.4.clone.rtab_hbm, f32[2,64,128]{2,1,0:T(8,128)} %constant.5.clone.ctab_hbm, bf16[1,128,1024]{2,1,0:T(8,128)(2,1)} %q_hbm.1, ...), custom_call_target="tpu_custom_call" | custom-call | tf_op jit(solution)/shard_map/layer/pallas_call | solution.py:526
  76.0 1.9 %copy.19 = bf16[1,128,2048]{2,1,0:T(8,128)(2,1)} copy(bf16[1,128,2048]{2,1,0:T(8,128)(2,1)} %layer.1) | data formatting | bytes 1048576

commit v6 on v5

--- a/solution.py
+++ b/solution.py
@@ -441,6 +441,21 @@
                         items += [(g, stage2(u, g, k1, True)) for k1 in NEAR + (0,)]
                 go(items)
 
+    def final(w):
+        for p in range(3):
+            drain(inboxr.at[w, :, pl.ds(0, 16), cols_of(p)], r1z.at[w * 3 + p])
+        for k1 in NEAR + (0,):
+            for p in range(3):
+                drain(inboxr.at[w, k1, pl.ds(16, 48), cols_of(p)], r2r.at[w * 3 + p, k1])
+                last1((w, p), k1).start()
+
+    def finish(*steps):
+        for step, w in steps:
+            if step == 2:
+                middle((w,))
+            else:
+                final(w)
+
     for turn_no in range(2):
         w = (1 - core + turn_no) % 2
         if turn_no == 0:
@@ -469,16 +484,9 @@
         if turn_no == 0:
             pl.when(core == 1)(lambda: middle((0,)))
         else:
-            pl.when(core == 1)(lambda: middle((1,)))
-            pl.when(core == 0)(lambda: middle((0, 1)))
-
-    for w in range(2):
-        for p in range(3):
-            drain(inboxr.at[w, :, pl.ds(0, 16), cols_of(p)], r1z.at[w * 3 + p])
-        for k1 in NEAR + (0,):
-            for p in range(3):
-                drain(inboxr.at[w, k1, pl.ds(16, 48), cols_of(p)], r2r.at[w * 3 + p, k1])
-                last1((w, p), k1).start()
+            pl.when(core == 1)(lambda: finish((2, 1), (3, 0), (3, 1)))
+            pl.when(core == 0)(lambda: finish((2, 0), (3, 0), (2, 1), (3, 1)))
+
 
     g0, g1 = [jnp.transpose(jnp.broadcast_to(gate_ref[k : k + 1, :], (128, 128))) for k in range(2)]
     sums = [None] * 3

time: 78.1 us -> 81.1 us (1.038)
  Pallas kernels: 76 us -> 79 us
    pallas_call x1, Pallas kernels: 76 us -> 79 us  [shards(): pl.pallas_call(kernel, out_shape=jax.ShapeDtypeStruct((1, TOK, D), BF16),...]
where the time goes in v6:
time: 81.1 us; the launch traced here: 80.9 us
  Pallas kernels  79 us (97%)
  local copies, waits for them, and re-layouts  1.88 us (2%)
    pallas_call x1, Pallas kernels, shards(): pl.pallas_call(kernel, out_shape=jax.ShapeDtypeStruct((1, TOK, D), BF16),...  79 us
    unnamed x1, local copies, waits for them, and re-layouts  1.88 us

profile of v6, /device:TPU:0, one launch (start us, length us, event | category | flops | bytes accessed | tf_op | source)
XLA Modules:
  0.0 80.9 jit_solution(6282501271873538586)
XLA Ops:
  0.0 79.0 %layer.1 = bf16[1,128,2048]{2,1,0:T(8,128)(2,1)} custom-call(bf16[1,128,256]{2,1,0:T(8,128)(2,1)} %k_hbm.1, bf16[1,128,256]{2,1,0:T(8,128)(2,1)} %v_hbm.1, f32[1,64]{1,0:T(1,128)} %bitcast.16, f32[16,8,128]{2,1,0:T(8,128)} %constant.4.clone.rtab_hbm, f32[2,64,128]{2,1,0:T(8,128)} %constant.5.clone.ctab_hbm, bf16[1,128,1024]{2,1,0:T(8,128)(2,1)} %q_hbm.1, ...), custom_call_target="tpu_custom_call" | custom-call | tf_op jit(solution)/shard_map/layer/pallas_call | solution.py:534
  79.0 1.9 %copy.19 = bf16[1,128,2048]{2,1,0:T(8,128)(2,1)} copy(bf16[1,128,2048]{2,1,0:T(8,128)(2,1)} %layer.1) | data formatting | bytes 1048576
